TPU v7x, 32 devices: a whole 2x2x4 slice. The times are simulated.
32 devices in a mesh: sp: 4 (over y, x), tp: 8 (over z, core).
Axes of the slice: x: 2, y: 2, z: 4, core: 2. Of those that a mesh axis runs over, the one named last changes fastest.
Arguments:
- query_rows: bfloat16 [8192, 1024], P('sp', 'tp'), may hold values from -6 to 6
- key_rows: bfloat16 [8192, 1024], P('sp', 'tp'), may hold values from -6 to 6
- value_rows: bfloat16 [8192, 1024], P('sp', 'tp'), may hold values from -6 to 6
- gate_rows: bfloat16 [8192, 1024], P('sp', 'tp'), may hold values from -6 to 6
- log_decay: float32 [16, 8192], P('tp', 'sp'), may hold values from -1 to 0
- residual: bfloat16 [8192, 2048], P(('sp', 'tp')), may hold values from -6 to 6
- head_gain: float32 [1024], P('tp'), may hold values from 0.1 to 1.9
- out_weight: bfloat16 [1024, 2048], P(None, 'tp'), may hold values from -0.1875 to 0.1875
- norm_gain: float32 [2048], replicated, may hold values from 0.1 to 1.9
- expert_ids: int32 [8192, 2], P(('sp', 'tp')), may hold values from 0 to 3, all different within a row; in each aligned block of 256 rows (0 to 255, 256 to 511, ...) at most 192 rows name the same one
- route_weights: float32 [8192, 2], P(('sp', 'tp')), may hold values from 0.2 to 1
- expert_gate: bfloat16 [2048, 4096], P(None, ('sp', 'tp')), may hold values from -0.125 to 0.125
- expert_up: bfloat16 [2048, 4096], P(None, ('sp', 'tp')), may hold values from -0.125 to 0.125
- expert_down: bfloat16 [2048, 4096], P(None, ('sp', 'tp')), may hold values from -0.1875 to 0.1875
- shared_gate: bfloat16 [2048, 512], replicated, may hold values from -0.125 to 0.125
- shared_up: bfloat16 [2048, 512], replicated, may hold values from -0.125 to 0.125
- shared_down: bfloat16 [2048, 512], replicated, may hold values from -0.25 to 0.25
Outputs:
- result: bfloat16 [8192, 2048], P(('sp', 'tp'))
Inputs may be any that keep to these rules, and one draw needn't show every extreme that they name: `expert_ids`: each row names 2 different experts. Within the rows of one device (aligned blocks of 256 rows) no expert is named by more than 192 rows, and in some block an expert is named by exactly 192 rows.
All inputs are finite; a program needn't handle non-finite values.
Results may differ from a plain program's by a relative error of at most 0.0075.
Values may be sent and summed in bfloat16 or wider, within the bound.
A program may use at most 128 MiB of HBM per device.

v0:
```python
import functools

import jax
import jax.numpy as jnp
from jax import lax
from jax.experimental import pallas as pl
from jax.experimental.pallas import tpu as pltpu
from jax.sharding import PartitionSpec as P


HEAD = 64
BLOCK = 256
EXTRA = 8


eps = 1e-05
F32 = jnp.float32
BF16 = jnp.bfloat16


def split(value):
    high = value.astype(BF16)
    return high, (value - high.astype(F32)).astype(BF16)


def per_head(columns, lanes):
    heads = columns.shape[1]
    out = jnp.broadcast_to(columns[:, 0:1], lanes.shape)
    for head in range(1, heads):
        out = jnp.where(lanes // HEAD == head, columns[:, head : head + 1], out)
    return out


def gathered_update(keys, values, column, lanes, end):
    scale = HEAD ** (-0.5)
    weighted = keys.astype(F32) * (jnp.exp(per_head(end - column, lanes)) * scale)
    high, low = split(weighted)
    dims = (((0,), (0,)), ((), ()))
    return lax.dot_general(high, values, dims, preferred_element_type=F32) + lax.dot_general(
        low, values, dims, preferred_element_type=F32
    )


def state_kernel(key_ref, value_ref, column_ref, out_ref):
    width = key_ref.shape[1]
    step = pl.program_id(0)

    @pl.when(step == 0)
    def _():
        out_ref[0:width, :] = jnp.zeros((width, width), F32)
        out_ref[width:, :] = jnp.zeros((EXTRA, width), F32)

    lanes = lax.broadcasted_iota(jnp.int32, key_ref.shape, 1)
    column = column_ref[...]
    end = column[BLOCK - 1 : BLOCK, :]
    end_lanes = per_head(end, lanes[0:1, :])
    fresh = gathered_update(key_ref[...], value_ref[...], column, lanes, end)
    out_ref[0:width, :] = out_ref[0:width, :] * jnp.exp(end_lanes) + fresh
    out_ref[width:, :] = out_ref[width:, :] + end_lanes


def retention_kernel(
    mine_ref, query_ref, key_ref, value_ref, gate_ref, column_ref, row_ref, gain_ref, states_ref,
    out_ref, state
):
    rows, width = query_ref.shape
    heads = width // HEAD
    step = pl.program_id(0)
    count = states_ref.shape[0]
    row_ids = lax.broadcasted_iota(jnp.int32, (width, width), 0) // HEAD
    column_ids = lax.broadcasted_iota(jnp.int32, (width, width), 1) // HEAD

    @pl.when(step == 0)
    def _():
        total = jnp.zeros((width, width), F32)
        for position in range(count - 1):
            decay = jnp.exp(states_ref[position, width : width + 1, :])
            longer = total * decay + states_ref[position, 0:width, :]
            total = jnp.where(position < mine_ref[0], longer, total)
        state[...] = jnp.where(row_ids == column_ids, total, 0.0)

    lanes = lax.broadcasted_iota(jnp.int32, (rows, width), 1)
    queries, keys, values = query_ref[...], key_ref[...], value_ref[...]
    column = column_ref[...]
    end = column[rows - 1 : rows, :]
    causal = lax.broadcasted_iota(jnp.int32, (rows, rows), 0) >= lax.broadcasted_iota(
        jnp.int32, (rows, rows), 1
    )
    scale = HEAD ** (-0.5)
    high, low = split(state[...])
    carried = jnp.dot(queries, high, preferred_element_type=F32) + jnp.dot(
        queries, low, preferred_element_type=F32
    )
    retained = carried * jnp.exp(per_head(column, lanes))
    inner = None
    for head in range(heads):
        own = jnp.where(lanes // HEAD == head, queries.astype(F32), 0.0).astype(BF16)
        scores = lax.dot_general(
            own, keys, (((1,), (1,)), ((), ())), preferred_element_type=F32
        )
        spread = column[:, head : head + 1] - row_ref[0, head : head + 1, :]
        damping = jnp.exp(jnp.where(causal, spread, -jnp.inf))
        factor = (scores * scale * damping).astype(BF16)
        term = jnp.dot(factor, values, preferred_element_type=F32)
        inner = term if inner is None else jnp.where(lanes // HEAD == head, term, inner)
    retained = retained + inner
    fresh = gathered_update(keys, values, column, lanes, end)
    end_lanes = per_head(end, lanes[0:1, :])
    state[...] = state[...] * jnp.exp(end_lanes) + jnp.where(row_ids == column_ids, fresh, 0.0)

    def head_mean(array):
        out = None
        for head in range(heads):
            inside = lanes // HEAD == head
            mean = jnp.sum(jnp.where(inside, array, 0.0), axis=1, keepdims=True) * (1.0 / HEAD)
            out = jnp.broadcast_to(mean, array.shape) if out is None else jnp.where(inside, mean, out)
        return out

    centered = retained - head_mean(retained)
    normed = centered * lax.rsqrt(head_mean(centered * centered) + eps)
    gates = gate_ref[...].astype(F32)
    out_ref[...] = (normed * gain_ref[...] * (gates * jax.nn.sigmoid(gates))).astype(BF16)


def retention(query_rows, key_rows, value_rows, gate_rows, log_decay, head_gain):
    rows, width = query_rows.shape
    heads = width // HEAD
    count = rows // BLOCK
    running = jnp.cumsum(log_decay.reshape(heads, count, BLOCK), axis=2)
    row = running.transpose(1, 0, 2)
    column = running.reshape(heads, rows).T
    block = pl.BlockSpec((BLOCK, width), lambda i: (i, 0))
    column_block = pl.BlockSpec((BLOCK, heads), lambda i: (i, 0))
    state_call = pl.pallas_call(
        state_kernel,
        grid=(count,),
        in_specs=[block, block, column_block],
        out_specs=pl.BlockSpec((width + EXTRA, width), lambda i: (0, 0)),
        out_shape=jax.ShapeDtypeStruct((width + EXTRA, width), F32),
        compiler_params=pltpu.CompilerParams(dimension_semantics=("arbitrary",)),
        cost_estimate=pl.CostEstimate(
            flops=4 * rows * width * width, bytes_accessed=4 * rows * width, transcendentals=rows * width
        ),
    )
    own = state_call(key_rows, value_rows, column)
    states = lax.all_gather(own, "sp")
    mine = lax.axis_index("sp").astype(jnp.int32).reshape(1)
    return pl.pallas_call(
        retention_kernel,
        grid=(count,),
        in_specs=[
            pl.BlockSpec(memory_space=pltpu.SMEM),
            block,
            block,
            block,
            block,
            column_block,
            pl.BlockSpec((1, heads, BLOCK), lambda i: (i, 0, 0)),
            pl.BlockSpec((1, width), lambda i: (0, 0)),
            pl.BlockSpec(states.shape, lambda i: (0, 0, 0)),
        ],
        out_specs=block,
        out_shape=jax.ShapeDtypeStruct((rows, width), BF16),
        scratch_shapes=[pltpu.VMEM((width, width), F32)],
        compiler_params=pltpu.CompilerParams(dimension_semantics=("arbitrary",)),
        cost_estimate=pl.CostEstimate(
            flops=8 * rows * width * BLOCK,
            bytes_accessed=10 * rows * width,
            transcendentals=rows * BLOCK * heads,
        ),
    )(mine, query_rows, key_rows, value_rows, gate_rows, column, row, head_gain[None, :], states)


def send(piece, pairs):
    return lax.ppermute(piece, "tp", pairs)


def ring_start(own):
    size = lax.axis_size("tp")
    right = [(i, (i + 2) % size) for i in range(size)]
    left = [(i, (i - 2) % size) for i in range(size)]
    swap = [(i, i ^ 1) for i in range(size)]
    return send(own, right), send(own, left), send(own, swap)


def ring_finish(own, from_left, from_right, other):
    size = lax.axis_size("tp")
    chips = size // 2
    right = [(i, (i + 2) % size) for i in range(size)]
    left = [(i, (i - 2) % size) for i in range(size)]
    swap = [(i, i ^ 1) for i in range(size)]
    half = own.shape[1] // 2
    last = chips // 2
    pieces = [[own], [other]]
    for hop in range(1, (chips - 1) // 2 + 1):
        if hop > 1:
            from_left = send(from_left, right)
            from_right = send(from_right, left)
        for piece in (from_left, from_right):
            pieces += [[piece], [send(piece, swap)]]
    if chips % 2 == 0 and last > 1:
        first = send(from_left[:, :half], right)
        second = send(from_right[:, half:], left)
        pieces += [[first, second], [send(first, swap), send(second, swap)]]
    elif chips == 2:
        pieces += [[from_left], [send(from_left, swap)]]
    return pieces


def expert_kernel(layout, row_ref, *refs):
    count = len(layout)
    piece_refs, out_ref = refs[:count], refs[count]
    weights, middle, sems = refs[count + 1 :]
    slots, _, width, ff = weights.shape
    rows = row_ref.shape[0]
    copies = []
    for index, (slot, start, length) in enumerate(layout):
        copy = pltpu.make_async_copy(
            piece_refs[index], weights.at[slot, :, pl.ds(start, length), :], sems.at[index]
        )
        copy.start()
        copies.append(copy)
    tile = rows // 2
    for pair in range(slots // 2):
        for index, (slot, _, _) in enumerate(layout):
            if slot // 2 == pair:
                copies[index].wait()

        @pl.loop(0, 2)
        def _(step):
            span = pl.ds(pl.multiple_of(step * tile, tile), tile)
            block = row_ref[span, :]
            gate = jnp.concatenate([weights[2 * pair, 0], weights[2 * pair + 1, 0]], axis=1)
            up = jnp.concatenate([weights[2 * pair, 1], weights[2 * pair + 1, 1]], axis=1)
            gated = jnp.dot(block, gate, preferred_element_type=F32)
            raised = jnp.dot(block, up, preferred_element_type=F32)
            value = gated * jax.nn.sigmoid(gated) * raised
            middle[span, 2 * pair * ff : 2 * (pair + 1) * ff] = value.astype(BF16)

    part = 512

    @pl.loop(0, width // part)
    def _(step):
        span = pl.ds(pl.multiple_of(step * part, part), part)
        down = jnp.concatenate([weights[slot, 2, span, :] for slot in range(slots)], axis=1)
        out_ref[:, span] = lax.dot_general(
            middle[...], down, (((1,), (1,)), ((), ())), preferred_element_type=F32
        ).astype(BF16)


def experts(rows, shards):
    _, width, ff = shards[0][0].shape
    count = len(shards)
    if ff % 128 or count % 2:
        whole = jnp.concatenate([jnp.concatenate(shard, axis=1) for shard in shards], axis=2)
        middle = (
            jax.nn.silu(jnp.dot(rows, whole[0], preferred_element_type=F32))
            * jnp.dot(rows, whole[1], preferred_element_type=F32)
        ).astype(BF16)
        return lax.dot_general(
            middle, whole[2], (((1,), (1,)), ((), ())), preferred_element_type=F32
        ).astype(BF16)
    layout, pieces = [], []
    for slot, shard in enumerate(shards):
        start = 0
        for piece in shard:
            layout.append((slot, start, piece.shape[1]))
            pieces.append(piece)
            start += piece.shape[1]
    return pl.pallas_call(
        functools.partial(expert_kernel, layout),
        in_specs=[pl.BlockSpec(memory_space=pltpu.VMEM)]
        + [pl.BlockSpec(memory_space=pl.ANY)] * len(pieces),
        out_specs=pl.BlockSpec(memory_space=pltpu.VMEM),
        out_shape=jax.ShapeDtypeStruct(rows.shape, BF16),
        scratch_shapes=[
            pltpu.VMEM((count, 3, width, ff), BF16),
            pltpu.VMEM((rows.shape[0], count * ff), BF16),
            pltpu.SemaphoreType.DMA((len(pieces),)),
        ],
        compiler_params=pltpu.CompilerParams(vmem_limit_bytes=60 * 1024 * 1024),
        cost_estimate=pl.CostEstimate(
            flops=6 * rows.shape[0] * width * count * ff,
            bytes_accessed=6 * width * count * ff + 4 * rows.size,
            transcendentals=rows.shape[0] * count * ff,
        ),
    )(rows, *pieces)


def on_device(
    query_rows,
    key_rows,
    value_rows,
    gate_rows,
    log_decay,
    residual,
    head_gain,
    out_weight,
    norm_gain,
    expert_ids,
    route_weights,
    expert_gate,
    expert_up,
    expert_down,
    shared_gate,
    shared_up,
    shared_down,
):
    part = out_weight.shape[0] // lax.axis_size("sp")
    own_part = lax.dynamic_slice_in_dim(out_weight, lax.axis_index("sp") * part, part, 0)
    out_part = lax.all_gather(own_part, "tp", axis=1, tiled=True)
    out_full = lax.all_gather(out_part, "sp", axis=0, tiled=True)
    shard = jnp.stack([expert_gate, expert_up, expert_down])
    shard, log_decay = lax.optimization_barrier((shard, log_decay))
    from_left, from_right, other = ring_start(shard)

    specialists = lax.axis_size("sp")
    tokens, chosen = expert_ids.shape
    width = residual.shape[1]
    capacity = 3 * tokens * chosen // (2 * specialists)
    names = jnp.arange(specialists, dtype=jnp.int32)[:, None]
    named = [expert_ids[:, j][None, :] == names for j in range(chosen)]
    match = functools.reduce(jnp.logical_or, named)
    weight = sum(jnp.where(named[j], route_weights[:, j][None, :], 0.0) for j in range(chosen))
    earlier = jnp.arange(tokens)[:, None] < jnp.arange(tokens)[None, :]
    position = jnp.dot(match.astype(BF16), earlier.astype(BF16), preferred_element_type=F32)
    place = jnp.where(match, position.astype(jnp.int32), -1)
    sits = place[:, None, :] == jnp.arange(capacity, dtype=jnp.int32)[None, :, None]
    pick = sits.astype(BF16).reshape(specialists * capacity, tokens)
    weight_high = lax.reduce_precision(weight, 8, 7)
    weight_low = weight - weight_high
    back_high = jnp.where(sits, weight_high[:, None, :], 0.0).astype(BF16)
    back_low = jnp.where(sits, weight_low[:, None, :], 0.0).astype(BF16)

    ret_rows = retention(query_rows, key_rows, value_rows, gate_rows, log_decay, head_gain)
    token_rows = lax.all_to_all(ret_rows, "tp", split_axis=0, concat_axis=1, tiled=True)
    token_rows, from_left, from_right = lax.optimization_barrier((token_rows, from_left, from_right))
    shards = ring_finish(shard, from_left, from_right, other)
    mixer = jnp.dot(token_rows, out_full, preferred_element_type=F32)
    hidden = (residual.astype(F32) + mixer).astype(BF16)
    hidden_wide = hidden.astype(F32)
    normed_rows = (
        hidden_wide
        * lax.rsqrt(jnp.mean(hidden_wide * hidden_wide, axis=1, keepdims=True) + eps)
        * norm_gain
    ).astype(BF16)
    outgoing = jnp.dot(pick, normed_rows, preferred_element_type=F32).astype(BF16)
    outgoing = outgoing.reshape(specialists, capacity, width)
    arrived = lax.all_to_all(outgoing, "sp", split_axis=0, concat_axis=0, tiled=True)
    shared_mid = (
        jax.nn.silu(jnp.dot(normed_rows, shared_gate, preferred_element_type=F32))
        * jnp.dot(normed_rows, shared_up, preferred_element_type=F32)
    ).astype(BF16)
    shared_out = lax.dot_general(
        shared_mid, shared_down, (((1,), (1,)), ((), ())), preferred_element_type=F32
    )
    flat_rows = arrived.reshape(-1, width)
    processed = experts(flat_rows, shards).reshape(arrived.shape)
    returned = lax.all_to_all(processed, "sp", split_axis=0, concat_axis=0, tiled=True)
    dims = (((0, 1), (0, 1)), ((), ()))
    routed = lax.dot_general(back_high, returned, dims, preferred_element_type=F32)
    routed += lax.dot_general(back_low, returned, dims, preferred_element_type=F32)
    return (hidden_wide + routed + shared_out).astype(BF16)


MESH = pl.DeviceIdType.MESH
NT = (((1,), (1,)), ((), ()))
TN = (((0,), (0,)), ((), ()))


def thirds(value):
    first = value.astype(BF16)
    rest = value - first.astype(F32)
    second = rest.astype(BF16)
    return first, second, (rest - second.astype(F32)).astype(BF16)


def layer_kernel(
    query_hbm, key_hbm, value_hbm, gate_hbm, decay_ref, residual_hbm, head_gain_ref, out_weight_hbm,
    norm_gain_ref, ids_ref, route_ref, expert_gate_hbm, expert_up_hbm, expert_down_hbm,
    shared_gate_hbm, shared_up_hbm, shared_down_hbm,
    result_ref,
    query, key, value, gates, residual, shared_gate, shared_up, shared_down,
    weights, out_full, running, row_running, updates, states, state, inner, ret_rows, token_rows,
    hidden, normed, squares, places, outgoing, arrived, middle, processed, returned, base,
    shared_middle, back,
    local_sem, state_send, state_recv, mix_send, mix_recv, out_z_send, out_xy_send, out_recv,
    out_pair_send, out_pair_recv, right_send, left_send, pair_send, weight_recv,
    go_send, go_recv, back_send, back_recv,
):
    places_count = states.shape[0]
    size = token_rows.shape[0]
    chips = size // 2
    sp = lax.axis_index("sp")
    tp = lax.axis_index("tp")
    z, core = tp // 2, tp % 2
    blocks, rows, width = ret_rows.shape
    heads = width // HEAD
    depth = residual.shape[1]
    capacity = arrived.shape[1]
    specialists = arrived.shape[0]
    ff = weights.shape[3]
    quarter = out_full.shape[1] // places_count
    out_columns = out_full.shape[2]
    pieces = returned.shape[0]
    piece = depth // pieces
    scale = HEAD ** (-0.5)
    inputs = (expert_gate_hbm, expert_up_hbm, expert_down_hbm)
    units = [(0, 0, depth), (1, 0, depth)] + [(2, index * piece, piece) for index in range(pieces)]

    def remote(src, dst, send, recv, device):
        return pltpu.make_async_remote_copy(
            src_ref=src, dst_ref=dst, send_sem=send, recv_sem=recv, device_id=device, device_id_type=MESH
        )

    partner = (sp, z * 2 + 1 - core)
    right = (sp, tp + 2)
    left = (sp, tp - 2)

    local = [
        pltpu.make_async_copy(src, dst, local_sem.at[index])
        for index, (src, dst) in enumerate(
            [
                (key_hbm, key),
                (value_hbm, value),
                (query_hbm, query),
                (gate_hbm, gates),
                (out_weight_hbm, out_full.at[tp]),
                (residual_hbm, residual),
                (shared_gate_hbm, shared_gate),
                (shared_up_hbm, shared_up),
                (shared_down_hbm, shared_down),
                (expert_gate_hbm, weights.at[tp, 0]),
                (expert_up_hbm, weights.at[tp, 1]),
                (expert_down_hbm, weights.at[tp, 2]),
            ]
        )
    ]
    for copy in local[:4]:
        copy.start()

    barrier = pltpu.get_barrier_semaphore()
    for step in range(1, size):
        pl.semaphore_signal(barrier, inc=1, device_id=(sp, (tp + step) % size), device_id_type=MESH)
    for step in range(1, places_count):
        pl.semaphore_signal(barrier, inc=1, device_id=(sp ^ step, tp), device_id_type=MESH)
    pl.semaphore_wait(barrier, size - 1 + places_count - 1)

    def weight_copy(slot, unit, send, device, own=False):
        which, start, length = units[unit]
        span = pl.ds(start, length)
        there = weights.at[slot, which, span, :]
        here = inputs[which].at[span, :] if own else there
        return remote(here, there, send, weight_recv.at[slot, unit], device)

    def own_send(unit):
        @pl.when(z < chips - 1)
        def _():
            weight_copy(tp, unit, right_send.at[z, unit], right, True).start()

        @pl.when(z > 0)
        def _():
            weight_copy(tp, unit, left_send.at[z, unit], left, True).start()

        weight_copy(tp, unit, pair_send.at[z, unit], partner, True).start()

    def relay(unit, distance):
        @pl.when(z - distance >= 0)
        def _():
            origin = z - distance
            slot = origin * 2 + core
            weight_copy(slot, unit, right_send.at[origin, unit], right).wait_recv()

            @pl.when(z < chips - 1)
            def _():
                weight_copy(slot, unit, right_send.at[origin, unit], right).start()

            weight_copy(slot, unit, pair_send.at[origin, unit], partner).start()

        @pl.when(z + distance < chips)
        def _():
            origin = z + distance
            slot = origin * 2 + core
            weight_copy(slot, unit, left_send.at[origin, unit], left).wait_recv()

            @pl.when(z > 0)
            def _():
                weight_copy(slot, unit, left_send.at[origin, unit], left).start()

            weight_copy(slot, unit, pair_send.at[origin, unit], partner).start()

    def from_partner(unit, chip):
        weight_copy(chip * 2 + 1 - core, unit, pair_send.at[chip, unit], partner).wait_recv()

    def out_z(step):
        target = (z + step) % chips
        span = pl.ds(pl.multiple_of(sp * quarter, quarter), quarter)
        return remote(
            out_weight_hbm.at[span, :], out_full.at[tp, span, :], out_z_send.at[step - 1],
            out_recv.at[tp, sp], (sp, target * 2 + core),
        )

    def out_piece(step, part, send, device):
        slot = ((z + step) % chips) * 2 + core
        span = pl.ds(pl.multiple_of(part * quarter, quarter), quarter)
        there = out_full.at[slot, span, :]
        return remote(there, there, send, out_recv.at[slot, part], device)

    def out_pair(slot, index, own=False):
        return remote(
            out_weight_hbm if own else out_full.at[slot], out_full.at[slot], out_pair_send.at[index],
            out_pair_recv.at[slot], partner,
        )

    for step in range(1, chips):
        out_z(step).start()
    own_send(0)
    out_pair(tp, 0, True).start()
    for copy in local[4:]:
        copy.start()

    row_ids = lax.broadcasted_iota(jnp.int32, (width, width), 0) // HEAD
    column_ids = lax.broadcasted_iota(jnp.int32, (width, width), 1) // HEAD
    same_head = row_ids == column_ids
    lanes = lax.broadcasted_iota(jnp.int32, (rows, width), 1)
    later = lax.broadcasted_iota(jnp.int32, (rows, rows), 0)
    sooner = lax.broadcasted_iota(jnp.int32, (rows, rows), 1)
    lower = jnp.where(later >= sooner, 1.0, 0.0).astype(BF16)
    upper = jnp.where(later <= sooner, 1.0, 0.0).astype(BF16)

    listed = jnp.concatenate(
        [
            decay_ref[head : head + 1, block * rows : (block + 1) * rows]
            for head in range(heads)
            for block in range(blocks)
        ],
        axis=0,
    )
    row_running[...] = functools.reduce(
        jnp.add, [jnp.dot(part, upper, preferred_element_type=F32) for part in thirds(listed)]
    )
    head_rows = lax.broadcasted_iota(jnp.int32, (width, rows), 0) // HEAD
    for block in range(blocks):
        spread = jnp.broadcast_to(listed[block : block + 1, :], (width, rows))
        for head in range(1, heads):
            spread = jnp.where(
                head_rows == head, listed[head * blocks + block : head * blocks + block + 1, :], spread
            )
        running[block] = functools.reduce(
            jnp.add,
            [
                lax.dot_general(lower, part, NT, preferred_element_type=F32)
                for part in thirds(spread)
            ],
        )

    for copy in local[:2]:
        copy.wait()
    state[...] = jnp.zeros((width + EXTRA, width), F32)

    @pl.loop(0, blocks)
    def _(block):
        span = pl.ds(pl.multiple_of(block * rows, rows), rows)
        column = running[block]
        end = column[rows - 1 : rows, :]
        weighted = key[span, :].astype(F32) * (jnp.exp(end - column) * scale)
        high, low = split(weighted)
        fresh = lax.dot_general(high, value[span, :], TN, preferred_element_type=F32)
        fresh += lax.dot_general(low, value[span, :], TN, preferred_element_type=F32)
        fresh = jnp.where(same_head, fresh, 0.0)
        updates[block] = fresh
        state[0:width, :] = state[0:width, :] * jnp.exp(end) + fresh
        state[width:, :] = state[width:, :] + end

    states[sp] = state[...]

    def state_copy(step):
        return remote(
            state, states.at[sp], state_send.at[step - 1], state_recv.at[sp], (sp ^ step, tp)
        )

    def state_arrival(step):
        return remote(
            state, states.at[sp ^ step], state_send.at[step - 1], state_recv.at[sp ^ step], (sp ^ step, tp)
        )

    local[2].wait()
    for step in range(1, places_count):
        state_copy(step).start()

    for step in range(1, chips):
        out_piece(step, sp, out_xy_send.at[step - 1, 0], partner).wait_recv()
        for other in range(1, places_count):
            out_piece(step, sp, out_xy_send.at[step - 1, other - 1], (sp ^ other, tp)).start()

    @pl.loop(0, blocks)
    def _(block):
        span = pl.ds(pl.multiple_of(block * rows, rows), rows)
        queries, keys, values = query[span, :], key[span, :], value[span, :]
        column = running[block]
        causal = later >= sooner
        total = None
        for head in range(heads):
            own = jnp.where(lanes // HEAD == head, queries.astype(F32), 0.0).astype(BF16)
            scores = lax.dot_general(own, keys, NT, preferred_element_type=F32)
            spread = column[:, head * HEAD : head * HEAD + 1] - row_running[pl.ds(head * blocks + block, 1), :]
            damping = jnp.exp(jnp.where(causal, spread, -jnp.inf))
            factor = (scores * scale * damping).astype(BF16)
            term = jnp.dot(factor, values, preferred_element_type=F32)
            total = term if total is None else jnp.where(lanes // HEAD == head, term, total)
        inner[block] = total

    for step in range(1, places_count):
        state_copy(step).wait_send()
        state_arrival(step).wait_recv()
    total = jnp.zeros((width, width), F32)
    for position in range(places_count - 1):
        longer = total * jnp.exp(states[position, width : width + 1, :]) + states[position, 0:width, :]
        total = jnp.where(position < sp, longer, total)
    state[0:width, :] = total
    local[3].wait()

    def head_mean(array):
        out = None
        for head in range(heads):
            inside = lanes // HEAD == head
            mean = jnp.sum(jnp.where(inside, array, 0.0), axis=1, keepdims=True) * (1.0 / HEAD)
            out = jnp.broadcast_to(mean, array.shape) if out is None else jnp.where(inside, mean, out)
        return out

    def mix_copy(block):
        return remote(
            ret_rows.at[block], token_rows.at[tp], mix_send.at[block], mix_recv.at[tp], (sp, block)
        )

    def mix_start(block):
        @pl.when(block != tp)
        def _():
            mix_copy(block).start()

    @pl.loop(0, blocks)
    def _(block):
        span = pl.ds(pl.multiple_of(block * rows, rows), rows)
        column = running[block]
        end = column[rows - 1 : rows, :]
        before = state[0:width, :]
        high, low = split(before)
        queries = query[span, :]
        carried = jnp.dot(queries, high, preferred_element_type=F32) + jnp.dot(
            queries, low, preferred_element_type=F32
        )
        state[0:width, :] = before * jnp.exp(end) + updates[block]
        retained = carried * jnp.exp(column) + inner[block]
        centered = retained - head_mean(retained)
        norm = centered * lax.rsqrt(head_mean(centered * centered) + eps)
        gate = gates[span, :].astype(F32)
        mixed = (norm * head_gain_ref[...] * (gate * jax.nn.sigmoid(gate))).astype(BF16)
        ret_rows[block] = mixed

        @pl.when(block == tp)
        def _():
            token_rows[tp] = mixed

        @pl.when(block > 0)
        def _():
            mix_start(block - 1)

    mix_start(blocks - 1)

    relay(0, 1)
    own_send(1)

    tokens = ids_ref.shape[0]
    chosen = ids_ref.shape[1]
    names = lax.broadcasted_iota(jnp.int32, (tokens, width), 1)
    ids = ids_ref[...]
    route = route_ref[...]
    match = names < 0
    weight = jnp.zeros((tokens, width), F32)
    for j in range(chosen):
        named = ids[:, j : j + 1] == names
        match = jnp.logical_or(match, named)
        weight = weight + jnp.where(named, route[:, j : j + 1], 0.0)
    strict = jnp.where(later > sooner, 1.0, 0.0).astype(BF16)
    position = jnp.dot(strict, jnp.where(match, 1.0, 0.0).astype(BF16), preferred_element_type=F32)
    place = jnp.where(match, position, -4096.0)
    places[...] = place.T[0 : places.shape[0], :]
    slots = lax.broadcasted_iota(jnp.int32, (tokens, specialists * capacity), 1).astype(F32)
    placed = jnp.zeros((tokens, specialists * capacity), F32)
    for index in range(specialists):
        spot = place[:, index : index + 1] + float(index * capacity)
        placed = jnp.where(slots == spot, weight[:, index : index + 1], placed)
    high, low = split(placed)
    back[0] = high
    back[1] = low

    for copy in local[4:6]:
        copy.wait()
    out_pair(tp, 0, True).wait_send()
    for step in range(1, chips):
        for other in range(1, places_count):
            out_piece(step, sp ^ other, out_xy_send.at[step - 1, other - 1], (sp ^ other, tp)).wait_recv()
        out_pair(((z + step) % chips) * 2 + core, step).start()
    for chip in range(chips):
        out_pair(chip * 2 + 1 - core, 0).wait_recv()
    for step in range(1, size):
        source = (tp + step) % size
        remote(
            ret_rows.at[0], token_rows.at[source], mix_send.at[0], mix_recv.at[source], (sp, source)
        ).wait_recv()

    squares[...] = jnp.zeros(squares.shape, F32)

    @pl.loop(0, size)
    def _(slot):
        span = pl.ds(pl.multiple_of(slot * out_columns, out_columns), out_columns)
        token = jnp.concatenate([token_rows[index] for index in range(size)], axis=1)
        mixer = jnp.dot(token, out_full[slot], preferred_element_type=F32)
        total = (residual[:, span].astype(F32) + mixer).astype(BF16)
        hidden[:, span] = total
        wide = total.astype(F32)
        wide = wide * wide
        squares[...] += functools.reduce(
            jnp.add, [wide[:, start : start + 128] for start in range(0, out_columns, 128)]
        )

    factor = lax.rsqrt(jnp.sum(squares[...], axis=1, keepdims=True) * (1.0 / depth) + eps)

    @pl.loop(0, depth // 256)
    def _(index):
        span = pl.ds(pl.multiple_of(index * 256, 256), 256)
        normed[:, span] = (hidden[:, span].astype(F32) * factor * norm_gain_ref[:, span]).astype(BF16)

    slot_rows = lax.broadcasted_iota(jnp.int32, (capacity, tokens), 0).astype(F32)

    def go(step):
        return remote(
            outgoing.at[step - 1], arrived.at[sp], go_send.at[step - 1], go_recv.at[sp], (sp ^ step, tp)
        )

    for step in list(range(places_count - 1, -1, -1)):
        sits = jnp.where(places[pl.ds(sp ^ step, 1), :] == slot_rows, 1.0, 0.0).astype(BF16)

        @pl.loop(0, depth // 512)
        def _(index):
            span = pl.ds(pl.multiple_of(index * 512, 512), 512)
            picked = jnp.dot(sits, normed[:, span], preferred_element_type=F32).astype(BF16)
            if step:
                outgoing[step - 1, :, span] = picked
            else:
                arrived[sp, :, span] = picked

        if step:
            go(step).start()

    relay(0, 2)
    relay(1, 1)

    for copy in local[6:9]:
        copy.wait()
    shared = shared_gate.shape[1]

    @pl.loop(0, shared // 256)
    def _(index):
        span = pl.ds(pl.multiple_of(index * 256, 256), 256)
        gated = jnp.dot(normed[...], shared_gate[:, span], preferred_element_type=F32)
        raised = jnp.dot(normed[...], shared_up[:, span], preferred_element_type=F32)
        shared_middle[:, span] = (gated * jax.nn.sigmoid(gated) * raised).astype(BF16)

    @pl.loop(0, depth // 512)
    def _(index):
        span = pl.ds(pl.multiple_of(index * 512, 512), 512)
        base[:, span] = hidden[:, span].astype(F32) + lax.dot_general(
            shared_middle[...], shared_down[span, :], NT, preferred_element_type=F32
        )

    relay(0, 3)
    relay(1, 2)
    for unit in range(2, len(units)):
        own_send(unit)

    for copy in local[9:]:
        copy.wait()
    for step in range(1, places_count):
        remote(
            outgoing.at[0], arrived.at[sp ^ step], go_send.at[0], go_recv.at[sp ^ step], (sp ^ step, tp)
        ).wait_recv()

    def pair_middle(chip):
        @pl.loop(0, specialists // 2)
        def _(index):
            rows_here = jnp.concatenate([arrived[2 * index], arrived[2 * index + 1]], axis=0)
            gate_pair = jnp.concatenate([weights[2 * chip, 0], weights[2 * chip + 1, 0]], axis=1)
            up_pair = jnp.concatenate([weights[2 * chip, 1], weights[2 * chip + 1, 1]], axis=1)
            gated = jnp.dot(rows_here, gate_pair, preferred_element_type=F32)
            raised = jnp.dot(rows_here, up_pair, preferred_element_type=F32)
            found = (gated * jax.nn.sigmoid(gated) * raised).astype(BF16)
            span = pl.ds(pl.multiple_of(index * 2 * capacity, 2 * capacity), 2 * capacity)
            middle[span, pl.ds(pl.multiple_of(chip * 2 * ff, 2 * ff), 2 * ff)] = found

    last_chip = jnp.where(z * 2 < chips, chips - 1, 0)

    def chip_at(index):
        if index == 0:
            return z
        if index == chips - 1:
            return last_chip
        toward = jnp.where(last_chip == 0, chips - 1 - index, index)
        shifted = jnp.where(last_chip == 0, chips - index, index - 1)
        passed = jnp.where(last_chip == 0, z <= chips - 1 - index, z >= index)
        return jnp.where(passed, shifted, toward)

    for index in range(chips):
        chip = chip_at(index)
        if index == chips - 1:
            relay(1, 3)
        for unit in (0, 1):
            from_partner(unit, chip)
        pair_middle(chip)

    def home(index, step, source):
        return remote(
            processed.at[index, source], returned.at[index, sp], back_send.at[index, step - 1],
            back_recv.at[index, sp], (source, tp),
        )

    for index in range(pieces):
        unit = 2 + index
        for distance in range(1, chips):
            relay(unit, distance)
        for chip in range(chips):
            from_partner(unit, chip)

        @pl.loop(0, piece // 256)
        def _(part):
            span = pl.ds(pl.multiple_of(index * piece + part * 256, 256), 256)
            down = jnp.concatenate([weights[slot, 2, span, :] for slot in range(size)], axis=1)
            columns = pl.ds(pl.multiple_of(part * 256, 256), 256)
            found = lax.dot_general(middle[...], down, NT, preferred_element_type=F32).astype(BF16)
            for source in range(specialists):
                own = found[source * capacity : (source + 1) * capacity, :]
                processed[index, source, :, columns] = own

                @pl.when(source == sp)
                def _():
                    returned[index, sp, :, columns] = own

        for step in range(1, places_count):
            home(index, step, sp ^ step).start()

    for index in range(pieces):
        for step in range(1, places_count):
            source = sp ^ step
            remote(
                processed.at[index, source], returned.at[index, source], back_send.at[index, step - 1],
                back_recv.at[index, source], (source, tp),
            ).wait_recv()

        rows_back = jnp.concatenate([returned[index, source] for source in range(specialists)], axis=0)
        routed = jnp.dot(back[0], rows_back, preferred_element_type=F32)
        routed += jnp.dot(back[1], rows_back, preferred_element_type=F32)
        span = slice(index * piece, (index + 1) * piece)
        result_ref[:, span] = (base[:, span] + routed).astype(BF16)

    for step in range(1, chips):
        out_z(step).wait_send()
        for other in range(1, places_count):
            out_piece(step, sp, out_xy_send.at[step - 1, other - 1], (sp ^ other, tp)).wait_send()
        out_pair(((z + step) % chips) * 2 + core, step).wait_send()

    @pl.loop(0, blocks)
    def _(block):
        @pl.when(block != tp)
        def _():
            mix_copy(block).wait_send()

    for step in range(1, places_count):
        go(step).wait_send()
        for index in range(pieces):
            home(index, step, sp ^ step).wait_send()
    for unit in range(len(units)):
        for origin in range(chips):
            slot = origin * 2 + core

            @pl.when(jnp.logical_and(origin <= z, z < chips - 1))
            def _():
                weight_copy(slot, unit, right_send.at[origin, unit], right).wait_send()

            @pl.when(jnp.logical_and(origin >= z, z > 0))
            def _():
                weight_copy(slot, unit, left_send.at[origin, unit], left).wait_send()

            weight_copy(slot, unit, pair_send.at[origin, unit], partner).wait_send()


def whole_layer(*arrays):
    (query, _, _, _, _, residual, head_gain, out_weight, norm_gain, ids, _, expert_gate) = arrays[:12]
    shared_gate = arrays[14]
    places_count, size = lax.axis_size("sp"), lax.axis_size("tp")
    rows_all, width = query.shape
    tokens, depth = residual.shape
    blocks = rows_all // tokens
    chosen = ids.shape[1]
    capacity = 3 * tokens * chosen // (2 * places_count)
    ff = expert_gate.shape[1]
    shared = shared_gate.shape[1]
    chips = size // 2
    pieces = 4
    units = 2 + pieces
    heads = width // HEAD
    dma = pltpu.SemaphoreType.DMA
    arrays = list(arrays)
    arrays[6] = head_gain[None, :]
    arrays[8] = norm_gain[None, :]
    small = (4, 6, 8, 9, 10)
    vmem, anywhere = pl.BlockSpec(memory_space=pltpu.VMEM), pl.BlockSpec(memory_space=pl.ANY)
    block = lambda *shape: pltpu.VMEM(shape, BF16)
    wide = lambda *shape: pltpu.VMEM(shape, F32)
    return pl.pallas_call(
        layer_kernel,
        in_specs=[vmem if index in small else anywhere for index in range(len(arrays))],
        out_specs=vmem,
        out_shape=jax.ShapeDtypeStruct((tokens, depth), BF16),
        scratch_shapes=[
            block(rows_all, width), block(rows_all, width), block(rows_all, width), block(rows_all, width),
            block(tokens, depth), block(depth, shared), block(depth, shared), block(depth, shared),
            block(size, 3, depth, ff),
            block(size, out_weight.shape[0], out_weight.shape[1]),
            wide(blocks, tokens, width),
            wide(heads * blocks, tokens),
            wide(blocks, width, width),
            wide(places_count, width + EXTRA, width),
            wide(width + EXTRA, width),
            wide(blocks, tokens, width),
            block(blocks, tokens, width),
            block(size, tokens, width),
            block(tokens, depth), block(tokens, depth),
            wide(tokens, 128),
            wide(8, tokens),
            block(places_count - 1, capacity, depth),
            block(places_count, capacity, depth),
            block(places_count * capacity, size * ff),
            block(pieces, places_count, capacity, depth // pieces),
            block(pieces, places_count, capacity, depth // pieces),
            wide(tokens, depth),
            block(tokens, shared),
            block(2, tokens, places_count * capacity),
            dma((12,)),
            dma((places_count - 1,)), dma((places_count,)),
            dma((blocks,)), dma((size,)),
            dma((chips - 1,)), dma((chips - 1, places_count - 1)), dma((size, places_count)),
            dma((chips,)), dma((size,)),
            dma((chips, units)), dma((chips, units)), dma((chips, units)), dma((size, units)),
            dma((places_count - 1,)), dma((places_count,)),
            dma((pieces, places_count - 1)), dma((pieces, places_count)),
        ],
        compiler_params=pltpu.CompilerParams(
            collective_id=0, has_side_effects=True, vmem_limit_bytes=66 * 1000 * 1000
        ),
        cost_estimate=pl.CostEstimate(
            flops=20 * 10**9, bytes_accessed=40 * 10**6, transcendentals=4 * 10**6
        ),
    )(*arrays)


def kernel_fits(mesh, shapes):
    places_count, size = mesh.shape["sp"], mesh.shape["tp"]
    if places_count != 4 or size % 2 or size < 4:
        return False
    width = shapes[0][1] // size
    tokens = shapes[5][0] // (places_count * size)
    rows_all = shapes[0][0] // places_count
    ff = shapes[11][1] // (places_count * size)
    return width == 128 and ff % 128 == 0 and tokens % 128 == 0 and rows_all == tokens * size


def solution(mesh):
    placed = (
        P("sp", "tp"),
        P("sp", "tp"),
        P("sp", "tp"),
        P("sp", "tp"),
        P("tp", "sp"),
        P(("sp", "tp"), None),
        P("tp"),
        P(None, "tp"),
        P(),
        P(("sp", "tp"), None),
        P(("sp", "tp"), None),
        P(None, ("sp", "tp")),
        P(None, ("sp", "tp")),
        P(None, ("sp", "tp")),
        P(),
        P(),
        P(),
    )

    placement = dict(mesh=mesh, in_specs=placed, out_specs=P(("sp", "tp"), None), check_vma=False)
    step = jax.shard_map(on_device, **placement)
    fused = jax.shard_map(whole_layer, **placement)

    def run(*arrays):
        fits = kernel_fits(mesh, [array.shape for array in arrays])
        return fused(*arrays) if fits else step(*arrays)

    return run
```

profile of v0, /device:TPU:0, one launch (start us, length us, event | category | flops | bytes accessed | tf_op | source)
XLA Modules:
  0.0 160.8 jit_solution(17109068616906102260)
XLA Ops:
  0.0 1.5 copy.18.ids_ref
  1.5 1.5 copy.19.route_ref
  2.9 155.5 %shard_map.163 = bf16[256,2048]{1,0:T(8,128)(2,1)} custom-call(bf16[2048,128]{1,0:T(8,128)(2,1)} %query_hbm.1, bf16[2048,128]{1,0:T(8,128)(2,1)} %key_hbm.1, bf16[2048,128]{1,0:T(8,128)(2,1)} %value_hbm.1, bf16[2048,128]{1,0:T(8,128)(2,1)} %gate_hbm.1, f32[2,2048]{1,0:T(2,128)} %decay_ref.1, bf16[256,2048]{1,0:T(8,128)(2,1)} %residual_hbm.1, ...), custom_call_target="tpu_custom_call" | custom-call | flops 20000000000 | bytes 40000000 | tf_op jit(solution)/shard_map/pallas_call | solution.py:919
  158.5 2.3 %copy.21 = bf16[256,2048]{1,0:T(8,128)(2,1)} copy(bf16[256,2048]{1,0:T(8,128)(2,1)} %shard_map.163) | data formatting | bytes 2097152
where the time goes:
time: 161 us
  Pallas kernels  156 us (97%)
  local copies, waits for them, and re-layouts  5.24 us (3%)
    pallas_call x1, Pallas kernels, whole_layer(): pl.pallas_call(layer_kernel, in_specs=[vmem if index in small else anywhe...  156 us
    unnamed x3, local copies, waits for them, and re-layouts  5.24 us

commit v1 on v0

--- a/solution.py
+++ b/solution.py
@@ -375,18 +375,24 @@
     return first, second, (rest - second.astype(F32)).astype(BF16)
 
 
+def piece_widths(depth):
+    return [128] + [256] * ((depth - 256) // 256) + [128]
+
+
 def layer_kernel(
-    query_hbm, key_hbm, value_hbm, gate_hbm, decay_ref, residual_hbm, head_gain_ref, out_weight_hbm,
-    norm_gain_ref, ids_ref, route_ref, expert_gate_hbm, expert_up_hbm, expert_down_hbm,
+    query_hbm, key_hbm, value_hbm, gate_hbm, decay_hbm, residual_hbm, head_gain_hbm, out_weight_hbm,
+    norm_gain_hbm, ids_hbm, route_hbm, expert_gate_hbm, expert_up_hbm, expert_down_hbm,
     shared_gate_hbm, shared_up_hbm, shared_down_hbm,
     result_ref,
+    decay_ref, head_gain_ref, norm_gain_ref, ids_ref, route_ref,
     query, key, value, gates, residual, shared_gate, shared_up, shared_down,
     weights, out_full, running, row_running, updates, states, state, inner, ret_rows, token_rows,
-    hidden, normed, squares, places, outgoing, arrived, middle, processed, returned, base,
-    shared_middle, back,
-    local_sem, state_send, state_recv, mix_send, mix_recv, out_z_send, out_xy_send, out_recv,
-    out_pair_send, out_pair_recv, right_send, left_send, pair_send, weight_recv,
-    go_send, go_recv, back_send, back_recv,
+    hidden, normed, squares, tables, outgoing, arrived, middle, processed, direct, passing, merged,
+    combined, final, base, shared_middle, back,
+    local_sem, state_send, state_recv, mix_send, mix_recv, out_z_send, out_xy_send, out_z_recv, out_xy_recv,
+    out_pair_send, out_pair_recv, right_send, left_send, pair_send, line_recv, pair_recv, pair_down_recv,
+    go_send, go_recv, table_send, table_recv, direct_send, direct_recv, passing_send, passing_recv,
+    merged_send, merged_recv, final_send, final_recv,
 ):
     places_count = states.shape[0]
     size = token_rows.shape[0]
@@ -402,11 +408,15 @@
     ff = weights.shape[3]
     quarter = out_full.shape[1] // places_count
     out_columns = out_full.shape[2]
-    pieces = returned.shape[0]
-    piece = depth // pieces
+    widths = piece_widths(depth)
+    pieces = len(widths)
+    starts = [sum(widths[:index]) for index in range(pieces)]
+    half = depth // 2
     scale = HEAD ** (-0.5)
     inputs = (expert_gate_hbm, expert_up_hbm, expert_down_hbm)
-    units = [(0, 0, depth), (1, 0, depth)] + [(2, index * piece, piece) for index in range(pieces)]
+    units = [(which, start, half) for which in (0, 1) for start in (0, half)]
+    first_down = len(units)
+    units += [(2, start, length) for start, length in zip(starts, widths)]
 
     def remote(src, dst, send, recv, device):
         return pltpu.make_async_remote_copy(
@@ -421,10 +431,15 @@
         pltpu.make_async_copy(src, dst, local_sem.at[index])
         for index, (src, dst) in enumerate(
             [
+                (decay_hbm, decay_ref),
+                (ids_hbm, ids_ref),
+                (route_hbm, route_ref),
                 (key_hbm, key),
                 (value_hbm, value),
                 (query_hbm, query),
                 (gate_hbm, gates),
+                (head_gain_hbm, head_gain_ref),
+                (norm_gain_hbm, norm_gain_ref),
                 (out_weight_hbm, out_full.at[tp]),
                 (residual_hbm, residual),
                 (shared_gate_hbm, shared_gate),
@@ -436,7 +451,7 @@
             ]
         )
     ]
-    for copy in local[:4]:
+    for copy in local[:9]:
         copy.start()
 
     barrier = pltpu.get_barrier_semaphore()
@@ -446,78 +461,110 @@
         pl.semaphore_signal(barrier, inc=1, device_id=(sp ^ step, tp), device_id_type=MESH)
     pl.semaphore_wait(barrier, size - 1 + places_count - 1)
 
-    def weight_copy(slot, unit, send, device, own=False):
+    def weight_copy(origin, unit, send, device, own=False, pair=False):
         which, start, length = units[unit]
         span = pl.ds(start, length)
-        there = weights.at[slot, which, span, :]
+        there = weights.at[origin * 2 + core, which, span, :]
         here = inputs[which].at[span, :] if own else there
-        return remote(here, there, send, weight_recv.at[slot, unit], device)
+        if not pair:
+            received = line_recv.at[origin, unit]
+        elif unit < first_down:
+            received = pair_recv.at[origin]
+        else:
+            received = pair_down_recv.at[unit - first_down]
+        return remote(here, there, send, received, device)
+
+    def to_partner(origin, unit, own=False):
+        return weight_copy(origin, unit, pair_send.at[origin], partner, own, True)
 
     def own_send(unit):
         @pl.when(z < chips - 1)
         def _():
-            weight_copy(tp, unit, right_send.at[z, unit], right, True).start()
+            weight_copy(z, unit, right_send.at[z], right, True).start()
 
         @pl.when(z > 0)
         def _():
-            weight_copy(tp, unit, left_send.at[z, unit], left, True).start()
-
-        weight_copy(tp, unit, pair_send.at[z, unit], partner, True).start()
+            weight_copy(z, unit, left_send.at[z], left, True).start()
+
+        to_partner(z, unit, True).start()
 
     def relay(unit, distance):
         @pl.when(z - distance >= 0)
         def _():
             origin = z - distance
-            slot = origin * 2 + core
-            weight_copy(slot, unit, right_send.at[origin, unit], right).wait_recv()
+            copy = weight_copy(origin, unit, right_send.at[origin], right)
+            copy.wait_recv()
 
             @pl.when(z < chips - 1)
             def _():
-                weight_copy(slot, unit, right_send.at[origin, unit], right).start()
-
-            weight_copy(slot, unit, pair_send.at[origin, unit], partner).start()
+                copy.start()
+
+            to_partner(origin, unit).start()
 
         @pl.when(z + distance < chips)
         def _():
             origin = z + distance
-            slot = origin * 2 + core
-            weight_copy(slot, unit, left_send.at[origin, unit], left).wait_recv()
+            copy = weight_copy(origin, unit, left_send.at[origin], left)
+            copy.wait_recv()
 
             @pl.when(z > 0)
             def _():
-                weight_copy(slot, unit, left_send.at[origin, unit], left).start()
-
-            weight_copy(slot, unit, pair_send.at[origin, unit], partner).start()
-
-    def from_partner(unit, chip):
-        weight_copy(chip * 2 + 1 - core, unit, pair_send.at[chip, unit], partner).wait_recv()
+                copy.start()
+
+            to_partner(origin, unit).start()
+
+    def from_partner(origin):
+        there = weights.at[0, 0:2]
+        remote(there, there, pair_send.at[origin], pair_recv.at[origin], partner).wait_recv()
+
+    def downs_from_partner(index):
+        there = weights.at[0, 2, pl.ds(0, chips * widths[index]), :]
+        remote(there, there, pair_send.at[0], pair_down_recv.at[index], partner).wait_recv()
 
     def out_z(step):
         target = (z + step) % chips
         span = pl.ds(pl.multiple_of(sp * quarter, quarter), quarter)
         return remote(
-            out_weight_hbm.at[span, :], out_full.at[tp, span, :], out_z_send.at[step - 1],
-            out_recv.at[tp, sp], (sp, target * 2 + core),
-        )
-
-    def out_piece(step, part, send, device):
-        slot = ((z + step) % chips) * 2 + core
-        span = pl.ds(pl.multiple_of(part * quarter, quarter), quarter)
-        there = out_full.at[slot, span, :]
-        return remote(there, there, send, out_recv.at[slot, part], device)
-
-    def out_pair(slot, index, own=False):
+            out_weight_hbm.at[span, :], out_full.at[tp, span, :], out_z_send, out_z_recv.at[z],
+            (sp, target * 2 + core),
+        )
+
+    def out_z_arrival(step):
+        origin = (z + step) % chips
+        there = out_full.at[0, pl.ds(0, quarter), :]
+        return remote(there, there, out_z_send, out_z_recv.at[origin], partner)
+
+    def out_piece(step, device):
+        origin = (z + step) % chips
+        span = pl.ds(pl.multiple_of(sp * quarter, quarter), quarter)
+        there = out_full.at[origin * 2 + core, span, :]
+        return remote(there, there, out_xy_send.at[step - 1], out_xy_recv.at[origin], device)
+
+    def out_pieces(step):
+        origin = (z + step) % chips
+        there = out_full.at[0, pl.ds(0, (places_count - 1) * quarter), :]
+        return remote(there, there, out_xy_send.at[step - 1], out_xy_recv.at[origin], partner)
+
+    def out_pair(slot, own=False):
         return remote(
-            out_weight_hbm if own else out_full.at[slot], out_full.at[slot], out_pair_send.at[index],
-            out_pair_recv.at[slot], partner,
-        )
+            out_weight_hbm if own else out_full.at[slot], out_full.at[slot], out_pair_send,
+            out_pair_recv, partner,
+        )
+
+    def out_pairs():
+        there = out_full.at[0:chips]
+        return remote(there, there, out_pair_send, out_pair_recv, partner)
 
     for step in range(1, chips):
         out_z(step).start()
     own_send(0)
-    out_pair(tp, 0, True).start()
-    for copy in local[4:]:
+    own_send(1)
+    out_pair(tp, True).start()
+    for copy in local[9:]:
         copy.start()
+
+    for copy in local[:3]:
+        copy.wait()
 
     row_ids = lax.broadcasted_iota(jnp.int32, (width, width), 0) // HEAD
     column_ids = lax.broadcasted_iota(jnp.int32, (width, width), 1) // HEAD
@@ -527,6 +574,24 @@
     sooner = lax.broadcasted_iota(jnp.int32, (rows, rows), 1)
     lower = jnp.where(later >= sooner, 1.0, 0.0).astype(BF16)
     upper = jnp.where(later <= sooner, 1.0, 0.0).astype(BF16)
+
+    chosen, tokens = ids_ref.shape
+    names = lax.broadcasted_iota(jnp.int32, (8, tokens), 0)
+    match = names < 0
+    weight = jnp.zeros((8, tokens), F32)
+    for j in range(chosen):
+        named = ids_ref[j : j + 1, :] == names
+        match = jnp.logical_or(match, named)
+        weight = weight + jnp.where(named, route_ref[j : j + 1, :], 0.0)
+    strict = jnp.where(later < sooner, 1.0, 0.0).astype(BF16)
+    position = jnp.dot(jnp.where(match, 1.0, 0.0).astype(BF16), strict, preferred_element_type=F32)
+    tables[0, 0:8, :] = jnp.where(match, position, -1.0)
+    tables[0, 8:16, :] = weight
+
+    def table_copy(step):
+        return remote(
+            tables.at[0], tables.at[step], table_send, table_recv.at[step - 1], (sp ^ step, tp)
+        )
 
     listed = jnp.concatenate(
         [
@@ -554,7 +619,7 @@
             ],
         )
 
-    for copy in local[:2]:
+    for copy in local[3:5]:
         copy.wait()
     state[...] = jnp.zeros((width + EXTRA, width), F32)
 
@@ -576,22 +641,19 @@
 
     def state_copy(step):
         return remote(
-            state, states.at[sp], state_send.at[step - 1], state_recv.at[sp], (sp ^ step, tp)
+            state, states.at[sp], state_send, state_recv.at[sp], (sp ^ step, tp)
         )
 
     def state_arrival(step):
         return remote(
-            state, states.at[sp ^ step], state_send.at[step - 1], state_recv.at[sp ^ step], (sp ^ step, tp)
-        )
-
-    local[2].wait()
+            state, states.at[sp ^ step], state_send, state_recv.at[sp ^ step], (sp ^ step, tp)
+        )
+
+    local[5].wait()
     for step in range(1, places_count):
         state_copy(step).start()
-
-    for step in range(1, chips):
-        out_piece(step, sp, out_xy_send.at[step - 1, 0], partner).wait_recv()
-        for other in range(1, places_count):
-            out_piece(step, sp, out_xy_send.at[step - 1, other - 1], (sp ^ other, tp)).start()
+    for step in (1, 2):
+        table_copy(step).start()
 
     @pl.loop(0, blocks)
     def _(block):
@@ -610,15 +672,22 @@
             total = term if total is None else jnp.where(lanes // HEAD == head, term, total)
         inner[block] = total
 
+    for step in range(1, chips):
+        out_z_arrival(step).wait_recv()
+        for other in range(1, places_count):
+            out_piece(step, (sp ^ other, tp)).start()
+
     for step in range(1, places_count):
-        state_copy(step).wait_send()
         state_arrival(step).wait_recv()
+    there = states.at[pl.ds(0, places_count - 1)]
+    remote(there, there, state_send, state_recv.at[0], partner).wait_send()
     total = jnp.zeros((width, width), F32)
     for position in range(places_count - 1):
         longer = total * jnp.exp(states[position, width : width + 1, :]) + states[position, 0:width, :]
         total = jnp.where(position < sp, longer, total)
     state[0:width, :] = total
-    local[3].wait()
+    local[6].wait()
+    local[7].wait()
 
     def head_mean(array):
         out = None
@@ -630,7 +699,7 @@
 
     def mix_copy(block):
         return remote(
-            ret_rows.at[block], token_rows.at[tp], mix_send.at[block], mix_recv.at[tp], (sp, block)
+            ret_rows.at[block], token_rows.at[tp], mix_send, mix_recv.at[tp], (sp, block)
         )
 
     def mix_start(block):
@@ -668,45 +737,35 @@
     mix_start(blocks - 1)
 
     relay(0, 1)
-    own_send(1)
-
-    tokens = ids_ref.shape[0]
-    chosen = ids_ref.shape[1]
-    names = lax.broadcasted_iota(jnp.int32, (tokens, width), 1)
-    ids = ids_ref[...]
-    route = route_ref[...]
-    match = names < 0
-    weight = jnp.zeros((tokens, width), F32)
-    for j in range(chosen):
-        named = ids[:, j : j + 1] == names
-        match = jnp.logical_or(match, named)
-        weight = weight + jnp.where(named, route[:, j : j + 1], 0.0)
-    strict = jnp.where(later > sooner, 1.0, 0.0).astype(BF16)
-    position = jnp.dot(strict, jnp.where(match, 1.0, 0.0).astype(BF16), preferred_element_type=F32)
-    place = jnp.where(match, position, -4096.0)
-    places[...] = place.T[0 : places.shape[0], :]
-    slots = lax.broadcasted_iota(jnp.int32, (tokens, specialists * capacity), 1).astype(F32)
-    placed = jnp.zeros((tokens, specialists * capacity), F32)
-    for index in range(specialists):
-        spot = place[:, index : index + 1] + float(index * capacity)
-        placed = jnp.where(slots == spot, weight[:, index : index + 1], placed)
-    high, low = split(placed)
-    back[0] = high
-    back[1] = low
-
-    for copy in local[4:6]:
+    own_send(2)
+    relay(1, 1)
+    own_send(3)
+
+    slot_rows = lax.broadcasted_iota(jnp.int32, (capacity, tokens), 0).astype(F32)
+    for step in (1, 2):
+        table_copy(step).wait_recv()
+    for turn, (table, pair) in enumerate(
+        ((0, (0, 2)), (0, (0, 1)), (1, (0, 2)), (2, (0, 1)), (0, (2, 3)))
+    ):
+        parts = []
+        for other in pair:
+            name = sp ^ other
+            place = tables[table, pl.ds(name, 1), :]
+            parts.append(jnp.where(place == slot_rows, tables[table, pl.ds(8 + name, 1), :], 0.0))
+        high, low = split(jnp.concatenate(parts, axis=0).T)
+        back[turn, 0] = high
+        back[turn, 1] = low
+
+    for copy in local[8:11]:
         copy.wait()
-    out_pair(tp, 0, True).wait_send()
     for step in range(1, chips):
-        for other in range(1, places_count):
-            out_piece(step, sp ^ other, out_xy_send.at[step - 1, other - 1], (sp ^ other, tp)).wait_recv()
-        out_pair(((z + step) % chips) * 2 + core, step).start()
-    for chip in range(chips):
-        out_pair(chip * 2 + 1 - core, 0).wait_recv()
+        out_pieces(step).wait_recv()
+        out_pair(((z + step) % chips) * 2 + core).start()
+    out_pairs().wait_recv()
     for step in range(1, size):
         source = (tp + step) % size
         remote(
-            ret_rows.at[0], token_rows.at[source], mix_send.at[0], mix_recv.at[source], (sp, source)
+            ret_rows.at[0], token_rows.at[source], mix_send, mix_recv.at[source], (sp, source)
         ).wait_recv()
 
     squares[...] = jnp.zeros(squares.shape, F32)
@@ -731,15 +790,15 @@
         span = pl.ds(pl.multiple_of(index * 256, 256), 256)
         normed[:, span] = (hidden[:, span].astype(F32) * factor * norm_gain_ref[:, span]).astype(BF16)
 
-    slot_rows = lax.broadcasted_iota(jnp.int32, (capacity, tokens), 0).astype(F32)
+    relay(0, 2)
 
     def go(step):
         return remote(
-            outgoing.at[step - 1], arrived.at[sp], go_send.at[step - 1], go_recv.at[sp], (sp ^ step, tp)
+            outgoing.at[step - 1], arrived.at[sp], go_send, go_recv.at[sp], (sp ^ step, tp)
         )
 
     for step in list(range(places_count - 1, -1, -1)):
-        sits = jnp.where(places[pl.ds(sp ^ step, 1), :] == slot_rows, 1.0, 0.0).astype(BF16)
+        sits = jnp.where(tables[0, pl.ds(sp ^ step, 1), :] == slot_rows, 1.0, 0.0).astype(BF16)
 
         @pl.loop(0, depth // 512)
         def _(index):
@@ -753,10 +812,10 @@
         if step:
             go(step).start()
 
-    relay(0, 2)
-    relay(1, 1)
-
-    for copy in local[6:9]:
+    relay(1, 2)
+    relay(2, 1)
+
+    for copy in local[11:14]:
         copy.wait()
     shared = shared_gate.shape[1]
 
@@ -775,15 +834,19 @@
         )
 
     relay(0, 3)
-    relay(1, 2)
-    for unit in range(2, len(units)):
-        own_send(unit)
-
-    for copy in local[9:]:
+    relay(3, 1)
+    relay(2, 2)
+    relay(1, 3)
+    relay(3, 2)
+    own_send(first_down)
+    own_send(first_down + 1)
+    own_send(first_down + 2)
+
+    for copy in local[14:]:
         copy.wait()
     for step in range(1, places_count):
         remote(
-            outgoing.at[0], arrived.at[sp ^ step], go_send.at[0], go_recv.at[sp ^ step], (sp ^ step, tp)
+            outgoing.at[0], arrived.at[sp ^ step], go_send, go_recv.at[sp ^ step], (sp ^ step, tp)
         ).wait_recv()
 
     def pair_middle(chip):
@@ -813,84 +876,150 @@
     for index in range(chips):
         chip = chip_at(index)
         if index == chips - 1:
-            relay(1, 3)
-        for unit in (0, 1):
-            from_partner(unit, chip)
+            relay(2, 3)
+            relay(3, 3)
+        from_partner(chip)
         pair_middle(chip)
 
-    def home(index, step, source):
+    tile = processed.shape[3]
+
+    def tiles(index):
+        return range(starts[index] // tile, (starts[index] + widths[index]) // tile)
+
+    def piece_of(number):
+        return next(index for index in range(pieces) if number in tiles(index))
+
+    def arrivals(buffer, send, received, index):
+        there = buffer.at[pl.ds(starts[index] // tile, widths[index] // tile)]
+        remote(there, there, send, received.at[index], partner).wait_recv()
+
+    def near(number):
+        return sp ^ (2, 1)[number % 2]
+
+    def far(number):
+        return sp ^ (1, 2)[number % 2]
+
+    def direct_copy(number):
         return remote(
-            processed.at[index, source], returned.at[index, sp], back_send.at[index, step - 1],
-            back_recv.at[index, sp], (source, tp),
-        )
-
-    for index in range(pieces):
-        unit = 2 + index
+            processed.at[number, near(number)], direct.at[number], direct_send,
+            direct_recv.at[piece_of(number)], (near(number), tp),
+        )
+
+    def passing_copy(number):
+        return remote(
+            processed.at[number, sp ^ 3], passing.at[number], passing_send,
+            passing_recv.at[piece_of(number)], (near(number), tp),
+        )
+
+    def merged_copy(number):
+        return remote(
+            merged.at[number], combined.at[number], merged_send,
+            merged_recv.at[piece_of(number)], (far(number), tp),
+        )
+
+    def weighted(turn, first, second):
+        rows_back = jnp.concatenate([first, second], axis=0)
+        return jnp.dot(back[turn, 0], rows_back, preferred_element_type=F32) + jnp.dot(
+            back[turn, 1], rows_back, preferred_element_type=F32
+        )
+
+    def merge(index):
+        arrivals(passing, passing_send, passing_recv, index)
+        for number in tiles(index):
+            found = weighted(2 + number % 2, processed[number, far(number)], passing[number])
+            merged[number] = found.astype(BF16)
+        for number in tiles(index):
+            merged_copy(number).start()
+
+    last_tile = depth // tile - 1
+
+    def final_copy(step):
+        return remote(
+            processed.at[last_tile, sp ^ step], final.at[step - 1], final_send, final_recv, (sp ^ step, tp)
+        )
+
+    def store(number, routed):
+        span = slice(number * tile, (number + 1) * tile)
+        result_ref[:, span] = (base[:, span] + routed).astype(BF16)
+
+    def combine(index):
+        arrivals(direct, direct_send, direct_recv, index)
+        arrivals(merged, merged_send, merged_recv, index)
+        for number in tiles(index):
+            routed = weighted(number % 2, processed[number, sp], direct[number])
+            store(number, routed + combined[number].astype(F32))
+
+    lead = 3
+    lag = 3
+    for turn in range(pieces + chips - 2):
+        if turn + lead < pieces:
+            own_send(first_down + turn + lead)
         for distance in range(1, chips):
-            relay(unit, distance)
-        for chip in range(chips):
-            from_partner(unit, chip)
-
-        @pl.loop(0, piece // 256)
-        def _(part):
-            span = pl.ds(pl.multiple_of(index * piece + part * 256, 256), 256)
-            down = jnp.concatenate([weights[slot, 2, span, :] for slot in range(size)], axis=1)
-            columns = pl.ds(pl.multiple_of(part * 256, 256), 256)
-            found = lax.dot_general(middle[...], down, NT, preferred_element_type=F32).astype(BF16)
+            if 0 <= turn - (distance - 1) < pieces:
+                relay(first_down + turn - (distance - 1), distance)
+        index = turn - (chips - 2)
+        if index < 0:
+            continue
+        downs_from_partner(index)
+        down = jnp.concatenate(
+            [weights[slot, 2, starts[index] : starts[index] + widths[index], :] for slot in range(size)], axis=1
+        )
+
+        found = lax.dot_general(middle[...], down, NT, preferred_element_type=F32).astype(BF16)
+        for part, number in enumerate(tiles(index)):
             for source in range(specialists):
-                own = found[source * capacity : (source + 1) * capacity, :]
-                processed[index, source, :, columns] = own
-
-                @pl.when(source == sp)
-                def _():
-                    returned[index, sp, :, columns] = own
-
-        for step in range(1, places_count):
-            home(index, step, sp ^ step).start()
-
-    for index in range(pieces):
-        for step in range(1, places_count):
-            source = sp ^ step
-            remote(
-                processed.at[index, source], returned.at[index, source], back_send.at[index, step - 1],
-                back_recv.at[index, source], (source, tp),
-            ).wait_recv()
-
-        rows_back = jnp.concatenate([returned[index, source] for source in range(specialists)], axis=0)
-        routed = jnp.dot(back[0], rows_back, preferred_element_type=F32)
-        routed += jnp.dot(back[1], rows_back, preferred_element_type=F32)
-        span = slice(index * piece, (index + 1) * piece)
-        result_ref[:, span] = (base[:, span] + routed).astype(BF16)
-
+                processed[number, source] = found[
+                    source * capacity : (source + 1) * capacity, part * tile : (part + 1) * tile
+                ]
+
+        if index == pieces - 1:
+            for step in range(places_count - 1, 0, -1):
+                final_copy(step).start()
+        else:
+            for number in tiles(index):
+                passing_copy(number).start()
+            for number in tiles(index):
+                direct_copy(number).start()
+        if index:
+            merge(index - 1)
+        if index >= lag:
+            combine(index - lag)
+
+    for index in range(pieces - lag, pieces - 1):
+        combine(index)
+    remote(final, final, final_send, final_recv, partner).wait_recv()
+    routed = weighted(1, processed[last_tile, sp], final[0]) + weighted(4, final[1], final[2])
+    store(last_tile, routed)
+
+    there = out_full.at[0, pl.ds(0, (chips - 1) * quarter), :]
+    remote(there, there, out_z_send, out_z_recv.at[0], partner).wait_send()
     for step in range(1, chips):
-        out_z(step).wait_send()
-        for other in range(1, places_count):
-            out_piece(step, sp, out_xy_send.at[step - 1, other - 1], (sp ^ other, tp)).wait_send()
-        out_pair(((z + step) % chips) * 2 + core, step).wait_send()
-
-    @pl.loop(0, blocks)
-    def _(block):
-        @pl.when(block != tp)
+        out_pieces(step).wait_send()
+    out_pairs().wait_send()
+    there = ret_rows.at[pl.ds(0, blocks - 1)]
+    remote(there, there, mix_send, mix_recv.at[0], partner).wait_send()
+    remote(outgoing, outgoing, go_send, go_recv.at[0], partner).wait_send()
+    for buffer, sent, received in (
+        (direct, direct_send, direct_recv), (passing, passing_send, passing_recv),
+        (merged, merged_send, merged_recv),
+    ):
+        there = buffer.at[pl.ds(0, last_tile)]
+        remote(there, there, sent, received.at[0], partner).wait_send()
+    remote(final, final, final_send, final_recv, partner).wait_send()
+    there = tables.at[0:2]
+    remote(there, there, table_send, table_recv.at[0], partner).wait_send()
+    for origin in range(chips):
+        there = weights.at[origin]
+
+        @pl.when(jnp.logical_and(origin <= z, z < chips - 1))
         def _():
-            mix_copy(block).wait_send()
-
-    for step in range(1, places_count):
-        go(step).wait_send()
-        for index in range(pieces):
-            home(index, step, sp ^ step).wait_send()
-    for unit in range(len(units)):
-        for origin in range(chips):
-            slot = origin * 2 + core
-
-            @pl.when(jnp.logical_and(origin <= z, z < chips - 1))
-            def _():
-                weight_copy(slot, unit, right_send.at[origin, unit], right).wait_send()
-
-            @pl.when(jnp.logical_and(origin >= z, z > 0))
-            def _():
-                weight_copy(slot, unit, left_send.at[origin, unit], left).wait_send()
-
-            weight_copy(slot, unit, pair_send.at[origin, unit], partner).wait_send()
+            remote(there, there, right_send.at[origin], line_recv.at[0, 0], right).wait_send()
+
+        @pl.when(jnp.logical_and(origin >= z, z > 0))
+        def _():
+            remote(there, there, left_send.at[origin], line_recv.at[0, 0], left).wait_send()
+
+        remote(there, there, pair_send.at[origin], line_recv.at[0, 0], partner).wait_send()
 
 
 def whole_layer(*arrays):
@@ -905,23 +1034,25 @@
     ff = expert_gate.shape[1]
     shared = shared_gate.shape[1]
     chips = size // 2
-    pieces = 4
-    units = 2 + pieces
+    pieces = len(piece_widths(depth))
+    units = 4 + pieces
     heads = width // HEAD
     dma = pltpu.SemaphoreType.DMA
     arrays = list(arrays)
     arrays[6] = head_gain[None, :]
     arrays[8] = norm_gain[None, :]
-    small = (4, 6, 8, 9, 10)
+    arrays[9], arrays[10] = arrays[9].T, arrays[10].T
     vmem, anywhere = pl.BlockSpec(memory_space=pltpu.VMEM), pl.BlockSpec(memory_space=pl.ANY)
     block = lambda *shape: pltpu.VMEM(shape, BF16)
     wide = lambda *shape: pltpu.VMEM(shape, F32)
     return pl.pallas_call(
         layer_kernel,
-        in_specs=[vmem if index in small else anywhere for index in range(len(arrays))],
+        in_specs=[anywhere] * len(arrays),
         out_specs=vmem,
-        out_shape=jax.ShapeDtypeStruct((tokens, depth), BF16),
+        out_shape=pltpu.VMEM((tokens, depth), BF16),
         scratch_shapes=[
+            wide(*arrays[4].shape), wide(1, width), wide(1, depth),
+            pltpu.VMEM(arrays[9].shape, jnp.int32), wide(*arrays[10].shape),
             block(rows_all, width), block(rows_all, width), block(rows_all, width), block(rows_all, width),
             block(tokens, depth), block(depth, shared), block(depth, shared), block(depth, shared),
             block(size, 3, depth, ff),
@@ -936,26 +1067,29 @@
             block(size, tokens, width),
             block(tokens, depth), block(tokens, depth),
             wide(tokens, 128),
-            wide(8, tokens),
+            wide(3, 16, tokens),
             block(places_count - 1, capacity, depth),
             block(places_count, capacity, depth),
             block(places_count * capacity, size * ff),
-            block(pieces, places_count, capacity, depth // pieces),
-            block(pieces, places_count, capacity, depth // pieces),
+            block(depth // 128, places_count, capacity, 128),
+            block(depth // 128, capacity, 128), block(depth // 128, capacity, 128),
+            block(depth // 128, tokens, 128), block(depth // 128, tokens, 128),
+            block(places_count - 1, capacity, 128),
             wide(tokens, depth),
             block(tokens, shared),
-            block(2, tokens, places_count * capacity),
-            dma((12,)),
-            dma((places_count - 1,)), dma((places_count,)),
-            dma((blocks,)), dma((size,)),
-            dma((chips - 1,)), dma((chips - 1, places_count - 1)), dma((size, places_count)),
-            dma((chips,)), dma((size,)),
-            dma((chips, units)), dma((chips, units)), dma((chips, units)), dma((size, units)),
-            dma((places_count - 1,)), dma((places_count,)),
-            dma((pieces, places_count - 1)), dma((pieces, places_count)),
+            block(5, 2, tokens, 2 * capacity),
+            dma((17,)),
+            dma, dma((places_count,)),
+            dma, dma((size,)),
+            dma, dma((chips - 1,)), dma((chips,)), dma((chips,)),
+            dma, dma,
+            dma((chips,)), dma((chips,)), dma((chips,)), dma((chips, units)), dma((chips,)), dma((pieces,)),
+            dma, dma((places_count,)),
+            dma, dma((2,)),
+            dma, dma((pieces,)), dma, dma((pieces,)), dma, dma((pieces,)), dma, dma,
         ],
         compiler_params=pltpu.CompilerParams(
-            collective_id=0, has_side_effects=True, vmem_limit_bytes=66 * 1000 * 1000
+            collective_id=0, has_side_effects=True, vmem_limit_bytes=58 * 1000 * 1000
         ),
         cost_estimate=pl.CostEstimate(
             flops=20 * 10**9, bytes_accessed=40 * 10**6, transcendentals=4 * 10**6

time: 161 us -> 142 us (0.88)
  Pallas kernels: 156 us -> 141 us
  local copies, waits for them, and re-layouts: 5.24 us -> 0.97 us
    pallas_call x1, Pallas kernels: 156 us -> 141 us  [whole_layer(): pl.pallas_call(layer_kernel, in_specs=[anywhere] * len(arrays), out_specs...]
    unnamed x3 -> x1, local copies, waits for them, and re-layouts: 5.24 us -> 0.97 us
where the time goes in v1:
time: 142 us
  Pallas kernels  141 us (99%)
    pallas_call x1, Pallas kernels, whole_layer(): pl.pallas_call(layer_kernel, in_specs=[anywhere] * len(arrays), out_specs...  141 us

profile of v1, /device:TPU:0, one launch (start us, length us, event | category | flops | bytes accessed | tf_op | source)
XLA Modules:
  0.0 141.9 jit_solution(1950908701873078335)
XLA Ops:
  0.0 140.9 %shard_map.163 = bf16[256,2048]{1,0:T(8,128)(2,1)S(1)} custom-call(bf16[2048,128]{1,0:T(8,128)(2,1)} %query_hbm.1, bf16[2048,128]{1,0:T(8,128)(2,1)} %key_hbm.1, bf16[2048,128]{1,0:T(8,128)(2,1)} %value_hbm.1, bf16[2048,128]{1,0:T(8,128)(2,1)} %gate_hbm.1, f32[2,2048]{1,0:T(2,128)} %decay_hbm.1, bf16[256,2048]{1,0:T(8,128)(2,1)} %residual_hbm.1, ...), custom_call_target="tpu_custom_call" | custom-call | flops 20000000000 | bytes 40000000 | tf_op jit(solution)/shard_map/pallas_call | solution.py:1048
  140.9 1.0 copy.19

commit v2 on v1

--- a/solution.py
+++ b/solution.py
@@ -388,7 +388,7 @@
     query, key, value, gates, residual, shared_gate, shared_up, shared_down,
     weights, out_full, running, row_running, updates, states, state, inner, ret_rows, token_rows,
     hidden, normed, squares, tables, outgoing, arrived, middle, processed, direct, passing, merged,
-    combined, final, base, shared_middle, back,
+    combined, final, base, shared_middle, back, shares,
     local_sem, state_send, state_recv, mix_send, mix_recv, out_z_send, out_xy_send, out_z_recv, out_xy_recv,
     out_pair_send, out_pair_recv, right_send, left_send, pair_send, line_recv, pair_recv, pair_down_recv,
     go_send, go_recv, table_send, table_recv, direct_send, direct_recv, passing_send, passing_recv,
@@ -412,6 +412,7 @@
     pieces = len(widths)
     starts = [sum(widths[:index]) for index in range(pieces)]
     half = depth // 2
+    tile = processed.shape[3]
     scale = HEAD ** (-0.5)
     inputs = (expert_gate_hbm, expert_up_hbm, expert_down_hbm)
     units = [(which, start, half) for which in (0, 1) for start in (0, half)]
@@ -451,14 +452,13 @@
             ]
         )
     ]
-    for copy in local[:9]:
-        copy.start()
-
     barrier = pltpu.get_barrier_semaphore()
     for step in range(1, size):
         pl.semaphore_signal(barrier, inc=1, device_id=(sp, (tp + step) % size), device_id_type=MESH)
     for step in range(1, places_count):
         pl.semaphore_signal(barrier, inc=1, device_id=(sp ^ step, tp), device_id_type=MESH)
+    for copy in local[:9]:
+        copy.start()
     pl.semaphore_wait(barrier, size - 1 + places_count - 1)
 
     def weight_copy(origin, unit, send, device, own=False, pair=False):
@@ -741,20 +741,54 @@
     relay(1, 1)
     own_send(3)
 
+    between = jnp.logical_and(z > 0, z < chips - 1)
+
+    @pl.when(jnp.logical_not(between))
+    def _():
+        for unit in range(first_down, len(units)):
+            own_send(unit)
+
+    def pass_on(unit, distance, rightward):
+        origin = z - distance if rightward else z + distance
+        sent, device = (right_send, right) if rightward else (left_send, left)
+        copy = weight_copy(origin, unit, sent.at[origin], device)
+        copy.wait_recv()
+        copy.start()
+        to_partner(origin, unit).start()
+
+    def inward(unit):
+        for chip, rightward in ((1, True), (chips - 2, False)):
+
+            @pl.when(z == chip)
+            def _():
+                sent, device = (right_send, right) if rightward else (left_send, left)
+                weight_copy(z, unit, sent.at[z], device, True).start()
+                to_partner(z, unit, True).start()
+                pass_on(unit, 1, rightward)
+
+    def outward(unit):
+        for chip, rightward in ((1, False), (chips - 2, True)):
+
+            @pl.when(z == chip)
+            def _():
+                sent, device = (right_send, right) if rightward else (left_send, left)
+                weight_copy(z, unit, sent.at[z], device, True).start()
+                for distance in (1, 2):
+                    pass_on(unit, distance, rightward)
+
+
     slot_rows = lax.broadcasted_iota(jnp.int32, (capacity, tokens), 0).astype(F32)
     for step in (1, 2):
         table_copy(step).wait_recv()
     for turn, (table, pair) in enumerate(
         ((0, (0, 2)), (0, (0, 1)), (1, (0, 2)), (2, (0, 1)), (0, (2, 3)))
     ):
-        parts = []
-        for other in pair:
+        for side, other in enumerate(pair):
             name = sp ^ other
             place = tables[table, pl.ds(name, 1), :]
-            parts.append(jnp.where(place == slot_rows, tables[table, pl.ds(8 + name, 1), :], 0.0))
-        high, low = split(jnp.concatenate(parts, axis=0).T)
-        back[turn, 0] = high
-        back[turn, 1] = low
+            back[turn, side] = jnp.where(place == slot_rows, 1.0, 0.0).T.astype(BF16)
+            share = tables[table, pl.ds(8 + name, 1), :]
+            shares[turn, side] = jnp.broadcast_to(share, (tile, tokens)).T
 
     for copy in local[8:11]:
         copy.wait()
@@ -838,9 +872,8 @@
     relay(2, 2)
     relay(1, 3)
     relay(3, 2)
-    own_send(first_down)
-    own_send(first_down + 1)
-    own_send(first_down + 2)
+    inward(first_down)
+    inward(first_down + 1)
 
     for copy in local[14:]:
         copy.wait()
@@ -848,6 +881,9 @@
         remote(
             outgoing.at[0], arrived.at[sp ^ step], go_send, go_recv.at[sp ^ step], (sp ^ step, tp)
         ).wait_recv()
+
+    outward(first_down)
+    inward(first_down + 2)
 
     def pair_middle(chip):
         @pl.loop(0, specialists // 2)
@@ -881,8 +917,6 @@
         from_partner(chip)
         pair_middle(chip)
 
-    tile = processed.shape[3]
-
     def tiles(index):
         return range(starts[index] // tile, (starts[index] + widths[index]) // tile)
 
@@ -918,10 +952,8 @@
         )
 
     def weighted(turn, first, second):
-        rows_back = jnp.concatenate([first, second], axis=0)
-        return jnp.dot(back[turn, 0], rows_back, preferred_element_type=F32) + jnp.dot(
-            back[turn, 1], rows_back, preferred_element_type=F32
-        )
+        first = jnp.dot(back[turn, 0], first, preferred_element_type=F32) * shares[turn, 0]
+        return first + jnp.dot(back[turn, 1], second, preferred_element_type=F32) * shares[turn, 1]
 
     def merge(index):
         arrivals(passing, passing_send, passing_recv, index)
@@ -949,17 +981,23 @@
             routed = weighted(number % 2, processed[number, sp], direct[number])
             store(number, routed + combined[number].astype(F32))
 
-    lead = 3
     lag = 3
-    for turn in range(pieces + chips - 2):
-        if turn + lead < pieces:
-            own_send(first_down + turn + lead)
-        for distance in range(1, chips):
-            if 0 <= turn - (distance - 1) < pieces:
-                relay(first_down + turn - (distance - 1), distance)
-        index = turn - (chips - 2)
-        if index < 0:
-            continue
+
+    outward(first_down + 1)
+    inward(first_down + 3)
+    for index in range(pieces):
+        unit = first_down + index
+
+        if index + 2 < pieces:
+            outward(unit + 2)
+        if index + 4 < pieces:
+            inward(unit + 4)
+
+        @pl.when(jnp.logical_not(between))
+        def _():
+            for distance in range(1, chips):
+                relay(unit, distance)
+
         downs_from_partner(index)
         down = jnp.concatenate(
             [weights[slot, 2, starts[index] : starts[index] + widths[index], :] for slot in range(size)], axis=1
@@ -1077,7 +1115,7 @@
             block(places_count - 1, capacity, 128),
             wide(tokens, depth),
             block(tokens, shared),
-            block(5, 2, tokens, 2 * capacity),
+            block(5, 2, tokens, capacity), wide(5, 2, tokens, 128),
             dma((17,)),
             dma, dma((places_count,)),
             dma, dma((size,)),
@@ -1099,7 +1137,7 @@
 
 def kernel_fits(mesh, shapes):
     places_count, size = mesh.shape["sp"], mesh.shape["tp"]
-    if places_count != 4 or size % 2 or size < 4:
+    if places_count != 4 or size != 8:
         return False
     width = shapes[0][1] // size
     tokens = shapes[5][0] // (places_count * size)

time: 142 us -> 138 us (0.972)
  Pallas kernels: 141 us -> 136 us
    pallas_call x1, Pallas kernels: 141 us -> 136 us  [whole_layer(): pl.pallas_call(layer_kernel, in_specs=[anywhere] * len(arrays), out_specs...]
where the time goes in v2:
time: 138 us; the launch traced here: 137 us
  Pallas kernels  136 us (99%)
    pallas_call x1, Pallas kernels, whole_layer(): pl.pallas_call(layer_kernel, in_specs=[anywhere] * len(arrays), out_specs...  136 us

profile of v2, /device:TPU:0, one launch (start us, length us, event | category | flops | bytes accessed | tf_op | source)
XLA Modules:
  0.0 137.4 jit_solution(9674642626105040042)
XLA Ops:
  0.0 136.5 %shard_map.163 = bf16[256,2048]{1,0:T(8,128)(2,1)S(1)} custom-call(bf16[2048,128]{1,0:T(8,128)(2,1)} %query_hbm.1, bf16[2048,128]{1,0:T(8,128)(2,1)} %key_hbm.1, bf16[2048,128]{1,0:T(8,128)(2,1)} %value_hbm.1, bf16[2048,128]{1,0:T(8,128)(2,1)} %gate_hbm.1, f32[2,2048]{1,0:T(2,128)} %decay_hbm.1, bf16[256,2048]{1,0:T(8,128)(2,1)} %residual_hbm.1, ...), custom_call_target="tpu_custom_call" | custom-call | flops 20000000000 | bytes 40000000 | tf_op jit(solution)/shard_map/pallas_call | solution.py:1086
  136.5 1.0 copy.19

commit v3 on v2

--- a/solution.py
+++ b/solution.py
@@ -392,7 +392,7 @@
     local_sem, state_send, state_recv, mix_send, mix_recv, out_z_send, out_xy_send, out_z_recv, out_xy_recv,
     out_pair_send, out_pair_recv, right_send, left_send, pair_send, line_recv, pair_recv, pair_down_recv,
     go_send, go_recv, table_send, table_recv, direct_send, direct_recv, passing_send, passing_recv,
-    merged_send, merged_recv, final_send, final_recv,
+    merged_send, merged_recv, final_send, final_recv, hello,
 ):
     places_count = states.shape[0]
     size = token_rows.shape[0]
@@ -453,13 +453,28 @@
         )
     ]
     barrier = pltpu.get_barrier_semaphore()
-    for step in range(1, size):
-        pl.semaphore_signal(barrier, inc=1, device_id=(sp, (tp + step) % size), device_id_type=MESH)
-    for step in range(1, places_count):
-        pl.semaphore_signal(barrier, inc=1, device_id=(sp ^ step, tp), device_id_type=MESH)
+
+    def greet(flag):
+        for step in (1, 2):
+            pl.semaphore_signal(flag, inc=1, device_id=(sp ^ step, tp), device_id_type=MESH)
+        pl.semaphore_signal(flag, inc=1, device_id=partner, device_id_type=MESH)
+
+        @pl.when(z < chips - 1)
+        def _():
+            pl.semaphore_signal(flag, inc=1, device_id=right, device_id_type=MESH)
+
+        @pl.when(z > 0)
+        def _():
+            pl.semaphore_signal(flag, inc=1, device_id=left, device_id_type=MESH)
+
+    def greeted(flag):
+        pl.semaphore_wait(flag, jnp.where(jnp.logical_or(z == 0, z == chips - 1), 4, 5))
+
+    greet(barrier)
     for copy in local[:9]:
         copy.start()
-    pl.semaphore_wait(barrier, size - 1 + places_count - 1)
+    greeted(barrier)
+    greet(hello.at[0])
 
     def weight_copy(origin, unit, send, device, own=False, pair=False):
         which, start, length = units[unit]
@@ -555,10 +570,15 @@
         there = out_full.at[0:chips]
         return remote(there, there, out_pair_send, out_pair_recv, partner)
 
-    for step in range(1, chips):
-        out_z(step).start()
+    @pl.when(z < chips - 1)
+    def _():
+        out_z(1).start()
+
+    @pl.when(z > 0)
+    def _():
+        out_z(chips - 1).start()
+
     own_send(0)
-    own_send(1)
     out_pair(tp, True).start()
     for copy in local[9:]:
         copy.start()
@@ -593,6 +613,8 @@
             tables.at[0], tables.at[step], table_send, table_recv.at[step - 1], (sp ^ step, tp)
         )
 
+    greeted(hello.at[0])
+    greet(hello.at[1])
     listed = jnp.concatenate(
         [
             decay_ref[head : head + 1, block * rows : (block + 1) * rows]
@@ -619,6 +641,21 @@
             ],
         )
 
+    greeted(hello.at[1])
+    greet(hello.at[2])
+
+    @pl.when(z == chips - 1)
+    def _():
+        out_z(1).start()
+
+    for step in range(2, chips - 1):
+        out_z(step).start()
+
+    @pl.when(z == 0)
+    def _():
+        out_z(chips - 1).start()
+
+    own_send(1)
     for copy in local[3:5]:
         copy.wait()
     state[...] = jnp.zeros((width + EXTRA, width), F32)
@@ -637,6 +674,7 @@
         state[0:width, :] = state[0:width, :] * jnp.exp(end) + fresh
         state[width:, :] = state[width:, :] + end
 
+    greeted(hello.at[2])
     states[sp] = state[...]
 
     def state_copy(step):
@@ -672,11 +710,6 @@
             total = term if total is None else jnp.where(lanes // HEAD == head, term, total)
         inner[block] = total
 
-    for step in range(1, chips):
-        out_z_arrival(step).wait_recv()
-        for other in range(1, places_count):
-            out_piece(step, (sp ^ other, tp)).start()
-
     for step in range(1, places_count):
         state_arrival(step).wait_recv()
     there = states.at[pl.ds(0, places_count - 1)]
@@ -736,17 +769,29 @@
 
     mix_start(blocks - 1)
 
-    relay(0, 1)
-    own_send(2)
-    relay(1, 1)
-    own_send(3)
-
     between = jnp.logical_and(z > 0, z < chips - 1)
 
     @pl.when(jnp.logical_not(between))
     def _():
-        for unit in range(first_down, len(units)):
+        for unit in range(2, len(units)):
             own_send(unit)
+
+    for step in range(1, chips):
+        out_z_arrival(step).wait_recv()
+        for other in range(1, places_count):
+            out_piece(step, (sp ^ other, tp)).start()
+
+    @pl.when(jnp.logical_not(between))
+    def _():
+        relay(0, 1)
+        relay(1, 1)
+
+    @pl.when(between)
+    def _():
+        relay(0, 1)
+        own_send(2)
+        relay(1, 1)
+        own_send(3)
 
     def pass_on(unit, distance, rightward):
         origin = z - distance if rightward else z + distance
@@ -1003,6 +1048,15 @@
             [weights[slot, 2, starts[index] : starts[index] + widths[index], :] for slot in range(size)], axis=1
         )
 
+        if index == pieces - 1:
+            for step in range(places_count - 1, -1, -1):
+                span = pl.ds(pl.multiple_of((sp ^ step) * capacity, capacity), capacity)
+                found = lax.dot_general(middle[span, :], down, NT, preferred_element_type=F32)
+                processed[last_tile, sp ^ step] = found.astype(BF16)
+                if step:
+                    final_copy(step).start()
+            merge(index - 1)
+            continue
         found = lax.dot_general(middle[...], down, NT, preferred_element_type=F32).astype(BF16)
         for part, number in enumerate(tiles(index)):
             for source in range(specialists):
@@ -1010,20 +1064,16 @@
                     source * capacity : (source + 1) * capacity, part * tile : (part + 1) * tile
                 ]
 
-        if index == pieces - 1:
-            for step in range(places_count - 1, 0, -1):
-                final_copy(step).start()
-        else:
-            for number in tiles(index):
-                passing_copy(number).start()
-            for number in tiles(index):
-                direct_copy(number).start()
+        for number in tiles(index):
+            passing_copy(number).start()
+        for number in tiles(index):
+            direct_copy(number).start()
         if index:
             merge(index - 1)
         if index >= lag:
             combine(index - lag)
 
-    for index in range(pieces - lag, pieces - 1):
+    for index in range(pieces - 1 - lag, pieces - 1):
         combine(index)
     remote(final, final, final_send, final_recv, partner).wait_recv()
     routed = weighted(1, processed[last_tile, sp], final[0]) + weighted(4, final[1], final[2])
@@ -1125,6 +1175,7 @@
             dma, dma((places_count,)),
             dma, dma((2,)),
             dma, dma((pieces,)), dma, dma((pieces,)), dma, dma((pieces,)), dma, dma,
+            pltpu.SemaphoreType.REGULAR((3,)),
         ],
         compiler_params=pltpu.CompilerParams(
             collective_id=0, has_side_effects=True, vmem_limit_bytes=58 * 1000 * 1000

time: 138 us -> 136 us (0.986)
    pallas_call x1, Pallas kernels: 136 us -> 135 us  [whole_layer(): pl.pallas_call(layer_kernel, in_specs=[anywhere] * len(arrays), out_specs...]
where the time goes in v3:
time: 136 us
  Pallas kernels  135 us (99%)
    pallas_call x1, Pallas kernels, whole_layer(): pl.pallas_call(layer_kernel, in_specs=[anywhere] * len(arrays), out_specs...  135 us

profile of v3, /device:TPU:0, one launch (start us, length us, event | category | flops | bytes accessed | tf_op | source)
XLA Modules:
  0.0 135.7 jit_solution(12656602492609096402)
XLA Ops:
  0.0 134.7 %shard_map.163 = bf16[256,2048]{1,0:T(8,128)(2,1)S(1)} custom-call(bf16[2048,128]{1,0:T(8,128)(2,1)} %query_hbm.1, bf16[2048,128]{1,0:T(8,128)(2,1)} %key_hbm.1, bf16[2048,128]{1,0:T(8,128)(2,1)} %value_hbm.1, bf16[2048,128]{1,0:T(8,128)(2,1)} %gate_hbm.1, f32[2,2048]{1,0:T(2,128)} %decay_hbm.1, bf16[256,2048]{1,0:T(8,128)(2,1)} %residual_hbm.1, ...), custom_call_target="tpu_custom_call" | custom-call | flops 20000000000 | bytes 40000000 | tf_op jit(solution)/shard_map/pallas_call | solution.py:1136
  134.7 1.0 copy.19

commit v4 on v3

--- a/solution.py
+++ b/solution.py
@@ -379,6 +379,9 @@
     return [128] + [256] * ((depth - 256) // 256) + [128]
 
 
+STRAIGHT = 1
+
+
 def layer_kernel(
     query_hbm, key_hbm, value_hbm, gate_hbm, decay_hbm, residual_hbm, head_gain_hbm, out_weight_hbm,
     norm_gain_hbm, ids_hbm, route_hbm, expert_gate_hbm, expert_up_hbm, expert_down_hbm,
@@ -391,8 +394,8 @@
     combined, final, base, shared_middle, back, shares,
     local_sem, state_send, state_recv, mix_send, mix_recv, out_z_send, out_xy_send, out_z_recv, out_xy_recv,
     out_pair_send, out_pair_recv, right_send, left_send, pair_send, line_recv, pair_recv, pair_down_recv,
-    go_send, go_recv, table_send, table_recv, direct_send, direct_recv, passing_send, passing_recv,
-    merged_send, merged_recv, final_send, final_recv, hello,
+    go_send, go_recv, table_send, table_recv, direct_send, home_recv, passing_send, passing_recv,
+    merged_send, final_send, final_recv, hello,
 ):
     places_count = states.shape[0]
     size = token_rows.shape[0]
@@ -477,12 +480,13 @@
     greet(hello.at[0])
 
     def weight_copy(origin, unit, send, device, own=False, pair=False):
+        rightward = device is right
         which, start, length = units[unit]
         span = pl.ds(start, length)
         there = weights.at[origin * 2 + core, which, span, :]
         here = inputs[which].at[span, :] if own else there
         if not pair:
-            received = line_recv.at[origin, unit]
+            received = line_recv.at[origin if rightward else origin - 1, unit]
         elif unit < first_down:
             received = pair_recv.at[origin]
         else:
@@ -490,16 +494,16 @@
         return remote(here, there, send, received, device)
 
     def to_partner(origin, unit, own=False):
-        return weight_copy(origin, unit, pair_send.at[origin], partner, own, True)
+        return weight_copy(origin, unit, pair_send, partner, own, True)
 
     def own_send(unit):
         @pl.when(z < chips - 1)
         def _():
-            weight_copy(z, unit, right_send.at[z], right, True).start()
+            weight_copy(z, unit, right_send, right, True).start()
 
         @pl.when(z > 0)
         def _():
-            weight_copy(z, unit, left_send.at[z], left, True).start()
+            weight_copy(z, unit, left_send, left, True).start()
 
         to_partner(z, unit, True).start()
 
@@ -507,7 +511,7 @@
         @pl.when(z - distance >= 0)
         def _():
             origin = z - distance
-            copy = weight_copy(origin, unit, right_send.at[origin], right)
+            copy = weight_copy(origin, unit, right_send, right)
             copy.wait_recv()
 
             @pl.when(z < chips - 1)
@@ -519,7 +523,7 @@
         @pl.when(z + distance < chips)
         def _():
             origin = z + distance
-            copy = weight_copy(origin, unit, left_send.at[origin], left)
+            copy = weight_copy(origin, unit, left_send, left)
             copy.wait_recv()
 
             @pl.when(z > 0)
@@ -530,11 +534,11 @@
 
     def from_partner(origin):
         there = weights.at[0, 0:2]
-        remote(there, there, pair_send.at[origin], pair_recv.at[origin], partner).wait_recv()
+        remote(there, there, pair_send, pair_recv.at[origin], partner).wait_recv()
 
     def downs_from_partner(index):
         there = weights.at[0, 2, pl.ds(0, chips * widths[index]), :]
-        remote(there, there, pair_send.at[0], pair_down_recv.at[index], partner).wait_recv()
+        remote(there, there, pair_send, pair_down_recv.at[index], partner).wait_recv()
 
     def out_z(step):
         target = (z + step) % chips
@@ -732,7 +736,7 @@
 
     def mix_copy(block):
         return remote(
-            ret_rows.at[block], token_rows.at[tp], mix_send, mix_recv.at[tp], (sp, block)
+            ret_rows.at[block], token_rows.at[tp], mix_send, mix_recv, (sp, block)
         )
 
     def mix_start(block):
@@ -796,7 +800,7 @@
     def pass_on(unit, distance, rightward):
         origin = z - distance if rightward else z + distance
         sent, device = (right_send, right) if rightward else (left_send, left)
-        copy = weight_copy(origin, unit, sent.at[origin], device)
+        copy = weight_copy(origin, unit, sent, device)
         copy.wait_recv()
         copy.start()
         to_partner(origin, unit).start()
@@ -807,7 +811,7 @@
             @pl.when(z == chip)
             def _():
                 sent, device = (right_send, right) if rightward else (left_send, left)
-                weight_copy(z, unit, sent.at[z], device, True).start()
+                weight_copy(z, unit, sent, device, True).start()
                 to_partner(z, unit, True).start()
                 pass_on(unit, 1, rightward)
 
@@ -817,7 +821,7 @@
             @pl.when(z == chip)
             def _():
                 sent, device = (right_send, right) if rightward else (left_send, left)
-                weight_copy(z, unit, sent.at[z], device, True).start()
+                weight_copy(z, unit, sent, device, True).start()
                 for distance in (1, 2):
                     pass_on(unit, distance, rightward)
 
@@ -841,11 +845,8 @@
         out_pieces(step).wait_recv()
         out_pair(((z + step) % chips) * 2 + core).start()
     out_pairs().wait_recv()
-    for step in range(1, size):
-        source = (tp + step) % size
-        remote(
-            ret_rows.at[0], token_rows.at[source], mix_send, mix_recv.at[source], (sp, source)
-        ).wait_recv()
+    there = token_rows.at[pl.ds(0, size - 1)]
+    remote(there, there, mix_send, mix_recv, partner).wait_recv()
 
     squares[...] = jnp.zeros(squares.shape, F32)
 
@@ -965,11 +966,19 @@
     def tiles(index):
         return range(starts[index] // tile, (starts[index] + widths[index]) // tile)
 
+    bent_tiles = depth // tile - STRAIGHT
+
+    def bent(index):
+        return [number for number in tiles(index) if number < bent_tiles]
+
+    def straight(index):
+        return [number for number in tiles(index) if number >= bent_tiles]
+
     def piece_of(number):
         return next(index for index in range(pieces) if number in tiles(index))
 
     def arrivals(buffer, send, received, index):
-        there = buffer.at[pl.ds(starts[index] // tile, widths[index] // tile)]
+        there = buffer.at[pl.ds(starts[index] // tile, len(bent(index)))]
         remote(there, there, send, received.at[index], partner).wait_recv()
 
     def near(number):
@@ -981,7 +990,7 @@
     def direct_copy(number):
         return remote(
             processed.at[number, near(number)], direct.at[number], direct_send,
-            direct_recv.at[piece_of(number)], (near(number), tp),
+            home_recv.at[piece_of(number)], (near(number), tp),
         )
 
     def passing_copy(number):
@@ -993,7 +1002,7 @@
     def merged_copy(number):
         return remote(
             merged.at[number], combined.at[number], merged_send,
-            merged_recv.at[piece_of(number)], (far(number), tp),
+            home_recv.at[piece_of(number)], (far(number), tp),
         )
 
     def weighted(turn, first, second):
@@ -1002,27 +1011,37 @@
 
     def merge(index):
         arrivals(passing, passing_send, passing_recv, index)
-        for number in tiles(index):
+        for number in bent(index):
             found = weighted(2 + number % 2, processed[number, far(number)], passing[number])
             merged[number] = found.astype(BF16)
-        for number in tiles(index):
+        for number in bent(index):
             merged_copy(number).start()
 
     last_tile = depth // tile - 1
 
-    def final_copy(step):
+    def final_copy(number, step):
+        turn = number - bent_tiles
         return remote(
-            processed.at[last_tile, sp ^ step], final.at[step - 1], final_send, final_recv, (sp ^ step, tp)
-        )
+            processed.at[number, sp ^ step], final.at[turn, step - 1], final_send, final_recv.at[turn],
+            (sp ^ step, tp),
+        )
+
+    def final_combine(number):
+        turn = number - bent_tiles
+        there = final.at[turn]
+        remote(there, there, final_send, final_recv.at[turn], partner).wait_recv()
+        routed = weighted(1, processed[number, sp], final[turn, 0])
+        store(number, routed + weighted(4, final[turn, 1], final[turn, 2]))
 
     def store(number, routed):
         span = slice(number * tile, (number + 1) * tile)
         result_ref[:, span] = (base[:, span] + routed).astype(BF16)
 
     def combine(index):
-        arrivals(direct, direct_send, direct_recv, index)
-        arrivals(merged, merged_send, merged_recv, index)
-        for number in tiles(index):
+        count = len(bent(index))
+        there = weights.at[0, 0, pl.ds(0, count * (capacity + tokens)), :]
+        remote(there, there, direct_send, home_recv.at[index], partner).wait_recv()
+        for number in bent(index):
             routed = weighted(number % 2, processed[number, sp], direct[number])
             store(number, routed + combined[number].astype(F32))
 
@@ -1054,7 +1073,7 @@
                 found = lax.dot_general(middle[span, :], down, NT, preferred_element_type=F32)
                 processed[last_tile, sp ^ step] = found.astype(BF16)
                 if step:
-                    final_copy(step).start()
+                    final_copy(last_tile, step).start()
             merge(index - 1)
             continue
         found = lax.dot_general(middle[...], down, NT, preferred_element_type=F32).astype(BF16)
@@ -1064,20 +1083,26 @@
                     source * capacity : (source + 1) * capacity, part * tile : (part + 1) * tile
                 ]
 
-        for number in tiles(index):
+        for number in straight(index):
+            final_copy(number, 3).start()
+        for number in bent(index):
             passing_copy(number).start()
-        for number in tiles(index):
+        for number in bent(index):
             direct_copy(number).start()
+        for number in straight(index):
+            final_copy(number, 2).start()
+            final_copy(number, 1).start()
         if index:
             merge(index - 1)
         if index >= lag:
             combine(index - lag)
 
-    for index in range(pieces - 1 - lag, pieces - 1):
+    for index in range(pieces - 1 - lag, pieces - 2):
         combine(index)
-    remote(final, final, final_send, final_recv, partner).wait_recv()
-    routed = weighted(1, processed[last_tile, sp], final[0]) + weighted(4, final[1], final[2])
-    store(last_tile, routed)
+    for number in range(bent_tiles, last_tile):
+        final_combine(number)
+    combine(pieces - 2)
+    final_combine(last_tile)
 
     there = out_full.at[0, pl.ds(0, (chips - 1) * quarter), :]
     remote(there, there, out_z_send, out_z_recv.at[0], partner).wait_send()
@@ -1085,29 +1110,27 @@
         out_pieces(step).wait_send()
     out_pairs().wait_send()
     there = ret_rows.at[pl.ds(0, blocks - 1)]
-    remote(there, there, mix_send, mix_recv.at[0], partner).wait_send()
+    remote(there, there, mix_send, mix_recv, partner).wait_send()
     remote(outgoing, outgoing, go_send, go_recv.at[0], partner).wait_send()
-    for buffer, sent, received in (
-        (direct, direct_send, direct_recv), (passing, passing_send, passing_recv),
-        (merged, merged_send, merged_recv),
-    ):
-        there = buffer.at[pl.ds(0, last_tile)]
-        remote(there, there, sent, received.at[0], partner).wait_send()
-    remote(final, final, final_send, final_recv, partner).wait_send()
+    for buffer, sent in ((direct, direct_send), (passing, passing_send), (merged, merged_send)):
+        there = buffer.at[pl.ds(0, bent_tiles)]
+        remote(there, there, sent, passing_recv.at[0], partner).wait_send()
+    remote(final, final, final_send, final_recv.at[0], partner).wait_send()
     there = tables.at[0:2]
     remote(there, there, table_send, table_recv.at[0], partner).wait_send()
-    for origin in range(chips):
-        there = weights.at[origin]
-
-        @pl.when(jnp.logical_and(origin <= z, z < chips - 1))
+    for chip in range(chips):
+
+        @pl.when(z == chip)
         def _():
-            remote(there, there, right_send.at[origin], line_recv.at[0, 0], right).wait_send()
-
-        @pl.when(jnp.logical_and(origin >= z, z > 0))
-        def _():
-            remote(there, there, left_send.at[origin], line_recv.at[0, 0], left).wait_send()
-
-        remote(there, there, pair_send.at[origin], line_recv.at[0, 0], partner).wait_send()
+            if chip < chips - 1:
+                there = weights.at[0 : chip + 1]
+                remote(there, there, right_send, line_recv.at[0, 0], right).wait_send()
+            if chip > 0:
+                there = weights.at[0 : chips - chip]
+                remote(there, there, left_send, line_recv.at[0, 0], left).wait_send()
+
+    there = weights.at[0:chips]
+    remote(there, there, pair_send, line_recv.at[0, 0], partner).wait_send()
 
 
 def whole_layer(*arrays):
@@ -1162,19 +1185,19 @@
             block(depth // 128, places_count, capacity, 128),
             block(depth // 128, capacity, 128), block(depth // 128, capacity, 128),
             block(depth // 128, tokens, 128), block(depth // 128, tokens, 128),
-            block(places_count - 1, capacity, 128),
+            block(STRAIGHT, places_count - 1, capacity, 128),
             wide(tokens, depth),
             block(tokens, shared),
             block(5, 2, tokens, capacity), wide(5, 2, tokens, 128),
             dma((17,)),
             dma, dma((places_count,)),
-            dma, dma((size,)),
+            dma, dma,
             dma, dma((chips - 1,)), dma((chips,)), dma((chips,)),
             dma, dma,
-            dma((chips,)), dma((chips,)), dma((chips,)), dma((chips, units)), dma((chips,)), dma((pieces,)),
+            dma, dma, dma, dma((chips - 1, units)), dma((chips,)), dma((pieces,)),
             dma, dma((places_count,)),
             dma, dma((2,)),
-            dma, dma((pieces,)), dma, dma((pieces,)), dma, dma((pieces,)), dma, dma,
+            dma, dma((pieces,)), dma, dma((pieces,)), dma, dma, dma((STRAIGHT,)),
             pltpu.SemaphoreType.REGULAR((3,)),
         ],
         compiler_params=pltpu.CompilerParams(

time: 136 us -> 135 us (level)
  no operation moved by 1% of the time
where the time goes in v4:
time: 135 us
  Pallas kernels  134 us (99%)
    pallas_call x1, Pallas kernels, whole_layer(): pl.pallas_call(layer_kernel, in_specs=[anywhere] * len(arrays), out_specs...  134 us

profile of v4, /device:TPU:0, one launch (start us, length us, event | category | flops | bytes accessed | tf_op | source)
XLA Modules:
  0.0 135.3 jit_solution(16932190007833401475)
XLA Ops:
  0.0 134.4 %shard_map.163 = bf16[256,2048]{1,0:T(8,128)(2,1)S(1)} custom-call(bf16[2048,128]{1,0:T(8,128)(2,1)} %query_hbm.1, bf16[2048,128]{1,0:T(8,128)(2,1)} %key_hbm.1, bf16[2048,128]{1,0:T(8,128)(2,1)} %value_hbm.1, bf16[2048,128]{1,0:T(8,128)(2,1)} %gate_hbm.1, f32[2,2048]{1,0:T(2,128)} %decay_hbm.1, bf16[256,2048]{1,0:T(8,128)(2,1)} %residual_hbm.1, ...), custom_call_target="tpu_custom_call" | custom-call | flops 20000000000 | bytes 40000000 | tf_op jit(solution)/shard_map/pallas_call | solution.py:1159
  134.4 1.0 copy.19

commit v5 on v4

--- a/solution.py
+++ b/solution.py
@@ -614,7 +614,7 @@
 
     def table_copy(step):
         return remote(
-            tables.at[0], tables.at[step], table_send, table_recv.at[step - 1], (sp ^ step, tp)
+            tables.at[0], tables.at[step], table_send, table_recv, (sp ^ step, tp)
         )
 
     greeted(hello.at[0])
@@ -683,12 +683,7 @@
 
     def state_copy(step):
         return remote(
-            state, states.at[sp], state_send, state_recv.at[sp], (sp ^ step, tp)
-        )
-
-    def state_arrival(step):
-        return remote(
-            state, states.at[sp ^ step], state_send, state_recv.at[sp ^ step], (sp ^ step, tp)
+            state, states.at[sp], state_send, state_recv, (sp ^ step, tp)
         )
 
     local[5].wait()
@@ -714,10 +709,8 @@
             total = term if total is None else jnp.where(lanes // HEAD == head, term, total)
         inner[block] = total
 
-    for step in range(1, places_count):
-        state_arrival(step).wait_recv()
     there = states.at[pl.ds(0, places_count - 1)]
-    remote(there, there, state_send, state_recv.at[0], partner).wait_send()
+    remote(there, there, state_send, state_recv, partner).wait()
     total = jnp.zeros((width, width), F32)
     for position in range(places_count - 1):
         longer = total * jnp.exp(states[position, width : width + 1, :]) + states[position, 0:width, :]
@@ -827,8 +820,8 @@
 
 
     slot_rows = lax.broadcasted_iota(jnp.int32, (capacity, tokens), 0).astype(F32)
-    for step in (1, 2):
-        table_copy(step).wait_recv()
+    there = tables.at[0:2]
+    remote(there, there, table_send, table_recv, partner).wait_recv()
     for turn, (table, pair) in enumerate(
         ((0, (0, 2)), (0, (0, 1)), (1, (0, 2)), (2, (0, 1)), (0, (2, 3)))
     ):
@@ -874,7 +867,7 @@
 
     def go(step):
         return remote(
-            outgoing.at[step - 1], arrived.at[sp], go_send, go_recv.at[sp], (sp ^ step, tp)
+            outgoing.at[step - 1], arrived.at[sp], go_send, go_recv, (sp ^ step, tp)
         )
 
     for step in list(range(places_count - 1, -1, -1)):
@@ -923,10 +916,8 @@
 
     for copy in local[14:]:
         copy.wait()
-    for step in range(1, places_count):
-        remote(
-            outgoing.at[0], arrived.at[sp ^ step], go_send, go_recv.at[sp ^ step], (sp ^ step, tp)
-        ).wait_recv()
+    there = arrived.at[pl.ds(0, places_count - 1)]
+    remote(there, there, go_send, go_recv, partner).wait_recv()
 
     outward(first_down)
     inward(first_down + 2)
@@ -1045,7 +1036,7 @@
             routed = weighted(number % 2, processed[number, sp], direct[number])
             store(number, routed + combined[number].astype(F32))
 
-    lag = 3
+    lag = 4
 
     outward(first_down + 1)
     inward(first_down + 3)
@@ -1111,13 +1102,13 @@
     out_pairs().wait_send()
     there = ret_rows.at[pl.ds(0, blocks - 1)]
     remote(there, there, mix_send, mix_recv, partner).wait_send()
-    remote(outgoing, outgoing, go_send, go_recv.at[0], partner).wait_send()
+    remote(outgoing, outgoing, go_send, go_recv, partner).wait_send()
     for buffer, sent in ((direct, direct_send), (passing, passing_send), (merged, merged_send)):
         there = buffer.at[pl.ds(0, bent_tiles)]
         remote(there, there, sent, passing_recv.at[0], partner).wait_send()
     remote(final, final, final_send, final_recv.at[0], partner).wait_send()
     there = tables.at[0:2]
-    remote(there, there, table_send, table_recv.at[0], partner).wait_send()
+    remote(there, there, table_send, table_recv, partner).wait_send()
     for chip in range(chips):
 
         @pl.when(z == chip)
@@ -1190,13 +1181,13 @@
             block(tokens, shared),
             block(5, 2, tokens, capacity), wide(5, 2, tokens, 128),
             dma((17,)),
-            dma, dma((places_count,)),
+            dma, dma,
             dma, dma,
             dma, dma((chips - 1,)), dma((chips,)), dma((chips,)),
             dma, dma,
             dma, dma, dma, dma((chips - 1, units)), dma((chips,)), dma((pieces,)),
-            dma, dma((places_count,)),
-            dma, dma((2,)),
+            dma, dma,
+            dma, dma,
             dma, dma((pieces,)), dma, dma((pieces,)), dma, dma, dma((STRAIGHT,)),
             pltpu.SemaphoreType.REGULAR((3,)),
         ],

time: 135 us -> 135 us (level)
  no operation moved by 1% of the time
where the time goes in v5:
time: 135 us
  Pallas kernels  134 us (99%)
    pallas_call x1, Pallas kernels, whole_layer(): pl.pallas_call(layer_kernel, in_specs=[anywhere] * len(arrays), out_specs...  134 us

profile of v5, /device:TPU:0, one launch (start us, length us, event | category | flops | bytes accessed | tf_op | source)
XLA Modules:
  0.0 135.3 jit_solution(17572066148854266043)
XLA Ops:
  0.0 134.3 %shard_map.163 = bf16[256,2048]{1,0:T(8,128)(2,1)S(1)} custom-call(bf16[2048,128]{1,0:T(8,128)(2,1)} %query_hbm.1, bf16[2048,128]{1,0:T(8,128)(2,1)} %key_hbm.1, bf16[2048,128]{1,0:T(8,128)(2,1)} %value_hbm.1, bf16[2048,128]{1,0:T(8,128)(2,1)} %gate_hbm.1, f32[2,2048]{1,0:T(2,128)} %decay_hbm.1, bf16[256,2048]{1,0:T(8,128)(2,1)} %residual_hbm.1, ...), custom_call_target="tpu_custom_call" | custom-call | flops 20000000000 | bytes 40000000 | tf_op jit(solution)/shard_map/pallas_call | solution.py:1150
  134.3 1.0 copy.19
